TPU v7x, 512 devices: a whole 4x4x16 slice. The times are simulated.
512 devices in a mesh: sp: 32 (over z, core), tp: 16 (over y, x).
Axes of the slice: x: 4, y: 4, z: 16, core: 2. Of those that a mesh axis runs over, the one named last changes fastest.
Arguments:
- resid: bfloat16 [6144, 2048], P('sp', 'tp'), may hold values from -12 to 12
- conv_value: bfloat16 [6144, 2048], P('sp', 'tp'), may hold values from -80 to 80
- conv_gate: bfloat16 [6144, 2048], P('sp', 'tp'), may hold values from -6 to 6
- depth_kernel: float32 [31, 2048], P(None, 'tp'), may hold values from -1 to 1
- chan_gain: float32 [2048], P('tp'), may hold values from 0.1 to 1.9
- point_weight: bfloat16 [2048, 2048], P('tp'), may hold values from -0.125 to 0.125
- mix_gain: float32 [2048], replicated, may hold values from 0.1 to 1.9
- out_weight: bfloat16 [2048, 2048], P(None, 'tp'), may hold values from -0.125 to 0.125
- norm_gain: float32 [2048], P('tp'), may hold values from 0.1 to 1.9
- route_ids: int32 [6144, 4], P('sp'), may hold values from 0 to 31, all different within a row; in each aligned block of 192 rows (0 to 191, 192 to 383, ...) at most 32 rows name the same one
- route_weights: float32 [6144, 4], P('sp'), may hold values from 0.05 to 0.5
- gate_experts: bfloat16 [32, 2048, 4096], P('sp', None, 'tp'), may hold values from -0.3125 to 0.3125
- up_experts: bfloat16 [32, 2048, 4096], P('sp', None, 'tp'), may hold values from -0.3125 to 0.3125
- down_experts: bfloat16 [32, 4096, 2048], P('sp', 'tp'), may hold values from -0.09375 to 0.09375
Outputs:
- result: bfloat16 [6144, 2048], P('sp', 'tp')
Inputs may be any that keep to these rules, and one draw needn't show every extreme that they name: `route_ids`: each row names 4 different experts; among the 192 rows of one index of sp no expert is named by more than 32 rows, and in some such block an expert is named by exactly 32.
All inputs are finite; a program needn't handle non-finite values.
Results may differ from a plain program's by a relative error of at most 0.024.
Values may be sent and summed in bfloat16 or wider, within the bound.
A program may use at most 64 MiB of HBM per device.

v0:
```python
import jax
import jax.numpy as jnp
from jax import lax
from jax.sharding import Mesh
from jax.sharding import PartitionSpec as P

E = 32
TOPK = 4
CAP = 32
TP = ("tp_0", "tp_1")


epsilon = 1e-05
clamp_limit = 7.0
swish_slope = 1.702


def from_behind(block, axis, distance):
    devices = range(lax.axis_size(axis))
    route = [(i - distance, i) for i in devices if i - distance in devices]
    return lax.ppermute(block, axis, route)


def over_axes(value, axes):
    for axis in axes:
        value = lax.psum(value, axis)
    return value


def split_up(value, dim, count):
    dims = value.shape
    pieces = value.reshape(*dims[:dim], count, dims[dim] // count, *dims[dim + 1 :])
    return jnp.moveaxis(pieces, dim, 0)


def summed_on_arrival(value, axis, dim):
    pieces = split_up(value, dim, lax.axis_size(axis))
    arrived = lax.all_to_all(pieces, axis, split_axis=0, concat_axis=0, tiled=True)
    return arrived.astype(jnp.float32).sum(axis=0)


def from_everyone(value, axis):
    copies = jnp.broadcast_to(value, (lax.axis_size(axis), *value.shape))
    return lax.all_to_all(copies, axis, split_axis=0, concat_axis=0, tiled=True)


def laid_out(pieces, dim):
    dims = list(pieces.shape[1:])
    dims[dim] *= pieces.shape[0]
    return jnp.moveaxis(pieces, 0, dim).reshape(dims)


def gathered_copies(value, axis, dim):
    pieces = from_everyone(value, axis)
    return laid_out(pieces, dim)


def shards(
    resid,
    conv_value,
    conv_gate,
    depth_kernel,
    chan_gain,
    point_weight,
    mix_gain,
    out_weight,
    norm_gain,
    route_ids,
    route_weights,
    gate_experts,
    up_experts,
    down_experts,
):
    tok_rows, chan_local = conv_value.shape
    feat_local = resid.shape[1]
    lookback = depth_kernel.shape[0] - 1
    gated = (conv_value.astype(jnp.float32) * jax.nn.sigmoid(conv_gate.astype(jnp.float32))).astype(
        jnp.bfloat16
    )
    earlier = from_behind(gated[tok_rows - lookback :], "sp", 1)
    padded = jnp.concatenate([earlier, gated], axis=0)
    conv = jnp.zeros((tok_rows, chan_local), jnp.float32)
    for tap in range(lookback + 1):
        conv = conv + padded[tap : tap + tok_rows].astype(jnp.float32) * depth_kernel[tap]
    chan_total = chan_local * lax.axis_size(TP)
    row_sums, row_squares = (
        over_axes(jnp.sum(conv, axis=1), TP),
        over_axes(jnp.sum(conv * conv, axis=1), TP),
    )
    row_mean = row_sums / chan_total
    row_var = row_squares / chan_total - row_mean * row_mean
    act = jax.nn.silu(
        (conv - row_mean[:, None]) * lax.rsqrt(row_var[:, None] + epsilon) * chan_gain
    ).astype(jnp.bfloat16)
    point = summed_on_arrival(
        jnp.dot(act, point_weight, preferred_element_type=jnp.float32).astype(jnp.bfloat16), TP, 0
    )
    mixed = (
        point * lax.rsqrt(jnp.mean(point * point, axis=1, keepdims=True) + epsilon) * mix_gain
    ).astype(jnp.bfloat16)
    branch = jnp.dot(gathered_copies(mixed, TP, 0), out_weight, preferred_element_type=jnp.float32)
    middle = (resid.astype(jnp.float32) + branch).astype(jnp.bfloat16)
    middle32 = middle.astype(jnp.float32)
    feat_total = feat_local * lax.axis_size(TP)
    squares = over_axes(jnp.sum(middle32 * middle32, axis=1), TP)
    normed = (middle32 * lax.rsqrt(squares[:, None] / feat_total + epsilon) * norm_gain).astype(
        jnp.bfloat16
    )
    flat_ids = route_ids.reshape(-1)
    expert_table = (flat_ids[:, None] == jnp.arange(E, dtype=jnp.int32)[None, :]).astype(jnp.int32)
    earlier_count = jnp.cumsum(expert_table, axis=0) - expert_table
    position = jnp.sum(earlier_count * expert_table, axis=1)
    slot_of = flat_ids * CAP + position
    slot_grid = slot_of.reshape(tok_rows, TOPK)
    picker = jnp.any(
        slot_grid[None, :, :] == jnp.arange(E * CAP, dtype=jnp.int32)[:, None, None], axis=2
    ).astype(jnp.bfloat16)
    outgoing = (
        jnp.dot(picker, normed, preferred_element_type=jnp.float32)
        .astype(jnp.bfloat16)
        .reshape(E, CAP, feat_local)
    )
    received = lax.all_gather(
        lax.all_to_all(outgoing, "sp", split_axis=0, concat_axis=0, tiled=True),
        TP,
        axis=2,
        tiled=True,
    )
    local_experts = gate_experts.shape[0]
    sources = received.shape[0] // local_experts
    count = received.shape[1]
    rows = received.reshape(sources, local_experts, count, received.shape[2])
    gate_pre = jnp.minimum(
        jnp.einsum("sjcd,jdf->sjcf", rows, gate_experts, preferred_element_type=jnp.float32),
        clamp_limit,
    )
    up_pre = jnp.clip(
        jnp.einsum("sjcd,jdf->sjcf", rows, up_experts, preferred_element_type=jnp.float32),
        -clamp_limit,
        clamp_limit,
    )
    hidden = (gate_pre * jax.nn.sigmoid(swish_slope * gate_pre) * (up_pre + 1.0)).astype(
        jnp.bfloat16
    )
    partial_value = jnp.einsum(
        "sjcf,jfd->sjcd", hidden, down_experts, preferred_element_type=jnp.float32
    )
    summed = summed_on_arrival(partial_value.astype(jnp.bfloat16), TP, 3).astype(jnp.bfloat16)
    returned = lax.all_to_all(
        summed.reshape(sources * local_experts, count, summed.shape[3]),
        "sp",
        split_axis=0,
        concat_axis=0,
        tiled=True,
    )
    flat_back = returned.reshape(E * CAP, feat_local)
    picked = flat_back[slot_of].astype(jnp.float32).reshape(tok_rows, TOPK, feat_local)
    routed_sum = jnp.sum(picked * route_weights[:, :, None], axis=1)
    return (middle32 + routed_sum).astype(jnp.bfloat16)


def solution(mesh):
    split = Mesh(mesh.devices.reshape(mesh.shape["sp"], 4, 4), ("sp", "tp_0", "tp_1"))
    return jax.shard_map(
        shards,
        mesh=split,
        in_specs=(
            P("sp", TP),
            P("sp", TP),
            P("sp", TP),
            P(None, TP),
            P(TP),
            P(TP, None),
            P(),
            P(None, TP),
            P(TP),
            P("sp", None),
            P("sp", None),
            P("sp", None, TP),
            P("sp", None, TP),
            P("sp", TP, None),
        ),
        out_specs=P("sp", TP),
        check_vma=False,
    )
```

profile of v0, /device:TPU:1, one launch (start us, length us, event | category | flops | bytes accessed | tf_op | source)
XLA Modules:
  0.0 313.9 jit_solution(2929535783332254951)
XLA Ops:
  6.5 0.9 multiply_convert_fusion.3
  7.5 4.9 %collective-permute-start = (bf16[30,128]{1,0:T(8,128)(2,1)S(1)}, bf16[30,128]{1,0:T(8,128)(2,1)S(1)}, u32[]{:S(2)}, u32[]{:S(2)}) collective-permute-start(bf16[30,128]{1,0:T(8,128)(2,1)S(1)} %slice.258), channel_id=1, source_target_pairs={{0,16},{16,32},{32,48},{48,64},{64,80},{80,96},{96,112},{112,128},... | collective-permute-start | bytes 23048 | tf_op jit(solution)/shard_map/ppermute | solution.py:21
  12.4 1.0 slice_bitcast_fusion.30
  13.4 1.0 slice_bitcast_fusion.29
  14.4 1.9 collective-permute-done
  16.3 0.5 fusion.66
  16.8 7.1 %all-reduce.1 = (f32[192]{0:T(256)S(1)}, f32[192]{0:T(256)S(1)}) all-reduce(f32[192]{0:T(256)S(1)} %get-tuple-element.6, f32[192]{0:T(256)S(1)} %get-tuple-element.5), channel_id=1, replica_groups=mesh['sp'=32,'tp_0'=4,'tp_1'=4] {'tp_0'}, use_global_device_ids=true, to_apply=%region_4.0 | all-reduce | flops 384 | bytes 3072 | tf_op jit(solution)/shard_map/psum | solution.py:26
  23.9 8.2 %all-reduce = (f32[192]{0:T(256)S(1)}, f32[192]{0:T(256)S(1)}) all-reduce(f32[192]{0:T(256)S(1)} %get-tuple-element.9, f32[192]{0:T(256)S(1)} %get-tuple-element.10), channel_id=1, replica_groups=mesh['sp'=32,'tp_0'=4,'tp_1'=4] {'tp_1'}, use_global_device_ids=true, to_apply=%region_5.0 | all-reduce | flops 384 | bytes 3072 | tf_op jit(solution)/shard_map/psum | solution.py:26
  32.1 1.5 convolution_convert_fusion
  33.6 1.2 reshape.122
  34.8 3.7 %all-to-all-start = ((bf16[16,12,2048]{2,1,0:T(8,128)(2,1)}), bf16[16,12,2048]{2,1,0:T(8,128)(2,1)S(1)}, u32[]{:S(2)}, u32[]{:S(2)}) async-start(bf16[16,12,2048]{2,1,0:T(8,128)(2,1)} %reshape.122), calls=%async_computation | async-start | bytes 2097152 | tf_op jit(solution)/shard_map/all_to_all | solution.py:38
  38.5 0.1 copy.28
  38.6 0.1 eq.42
  38.7 0.1 eq.38
  38.8 14.4 %all-to-all-done = bf16[16,12,2048]{2,1,0:T(8,128)(2,1)S(1)} async-done(((bf16[16,12,2048]{2,1,0:T(8,128)(2,1)}), bf16[16,12,2048]{2,1,0:T(8,128)(2,1)S(1)}, u32[]{:S(2)}, u32[]{:S(2)}) %all-to-all-start) | async-done | bytes 786464 | tf_op jit(solution)/shard_map/all_to_all | solution.py:38
  53.2 0.2 convert_reduce_fusion
  53.4 0.1 multiply_reduce_fusion
  53.5 0.1 multiply_convert_fusion
  53.6 1.1 broadcast_in_dim.2
  54.7 3.7 %all-to-all-start.1 = ((bf16[16,12,2048]{2,1,0:T(8,128)(2,1)}), bf16[16,12,2048]{2,1,0:T(8,128)(2,1)S(1)}, u32[]{:S(2)}, u32[]{:S(2)}) async-start(bf16[16,12,2048]{2,1,0:T(8,128)(2,1)} %broadcast_in_dim.2), calls=%async_computation.1 | async-start | bytes 2097152 | tf_op jit(solution)/shard_map/all_to_all | solution.py:44
  58.5 0.0 all-gather.2.cloned.1.call-start
  58.5 1.7 reduce-window.6
  60.3 0.3 slice_reduce_fusion
  60.6 0.1 fusion.22
  60.7 0.6 copy-done.3
  61.3 0.1 reduce_sum.84
  61.4 0.1 copy.32
  61.5 1.2 fusion
  62.7 9.5 %all-to-all-done.1 = bf16[16,12,2048]{2,1,0:T(8,128)(2,1)S(1)} async-done(((bf16[16,12,2048]{2,1,0:T(8,128)(2,1)}), bf16[16,12,2048]{2,1,0:T(8,128)(2,1)S(1)}, u32[]{:S(2)}, u32[]{:S(2)}) %all-to-all-start.1) | async-done | bytes 786464 | tf_op jit(solution)/shard_map/all_to_all | solution.py:44
  72.2 0.2 reshape.123
  72.4 0.5 multiply_reduce_fusion.1
  72.8 7.3 %psum.46 = f32[192]{0:T(256)S(1)} all-reduce(f32[192]{0:T(256)S(1)} %get-tuple-element.47), channel_id=1, replica_groups=mesh['sp'=32,'tp_0'=4,'tp_1'=4] {'tp_0'}, use_global_device_ids=true, to_apply=%region_13.14 | all-reduce | flops 192 | bytes 1536 | tf_op jit(solution)/shard_map/psum | solution.py:26
  80.1 6.6 %psum.47 = f32[192]{0:T(256)S(1)} all-reduce(f32[192]{0:T(256)S(1)} %psum.46), channel_id=1, replica_groups=mesh['sp'=32,'tp_0'=4,'tp_1'=4] {'tp_1'}, use_global_device_ids=true, to_apply=%region_14.15 | all-reduce | flops 192 | bytes 1536 | tf_op jit(solution)/shard_map/psum | solution.py:26
  86.7 1.4 convolution_convert_fusion.1
  88.2 44.7 %all_to_all.25 = bf16[32,32,128]{2,1,0:T(8,128)(2,1)} all-to-all(bf16[32,32,128]{2,1,0:T(8,128)(2,1)S(1)} %bitcast.146), channel_id=1, replica_groups=mesh['sp'=32,'tp_0'=4,'tp_1'=4] {'sp'}, dimensions={0} | all-to-all | bytes 524288 | tf_op jit(solution)/shard_map/all_to_all | solution.py:124
  132.9 58.5 %all-gather.2.cloned.1.call-done = bf16[32,32,2048]{2,1,0:T(8,128)(2,1)} async-done(((bf16[32,32,128]{2,1,0:T(8,128)(2,1)}), bf16[32,32,2048]{2,1,0:T(8,128)(2,1)}) %all-gather.2.cloned.1.call-update) | async-done | bytes 4194320 | tf_op jit(solution)/shard_map/all_gather | solution.py:123
  191.4 4.8 %fusion.1 = f32[32,1,32,256]{3,2,0,1:T(8,128)} fusion(bf16[32,32,2048]{2,1,0:T(8,128)(2,1)} %all-gather.2.cloned.1.call-done, bf16[1,2048,256]{2,1,0:T(8,128)(2,1)} %param.25), kind=kOutput, calls=%fused_computation.8 | convolution fusion | flops 1074003968 | bytes 6291456 | tf_op jit(solution)/shard_map/sjcd,jdf->sjcf/dot_general | solution.py:134
  196.2 8.9 %convert_bitcast_fusion = bf16[1,32,4,16,8,128]{5,4,3,2,1,0:T(8,128)(2,1)} fusion(bf16[1,256,2048]{2,1,0:T(8,128)(2,1)S(1)} %copy-done, bf16[32,32,2048]{2,1,0:T(8,128)(2,1)} %all-gather.2.cloned.1.call-done, bf16[1,2048,256]{2,1,0:T(8,128)(2,1)S(1)} %copy-done.8, f32[32,1,32,256]{3,2,0,1:T(8,128)} %fusion.1), kind=kOutput, calls=%fused_computation.2 | convolution fusion | flops 2151940096 | bytes 11534336 | tf_op jit(solution)/shard_map/sjcf,jfd->sjcd/dot_general | solution.py:145
  205.1 3.3 %copy.39 = bf16[1,32,4,16,8,128]{5,4,2,1,0,3:T(8,128)(2,1)S(1)} copy(bf16[1,32,4,16,8,128]{5,4,3,2,1,0:T(8,128)(2,1)} %convert_bitcast_fusion) | data formatting | bytes 8388608 | tf_op jit(solution)/shard_map/reshape | solution.py:32
  208.4 54.5 %all_to_all.26 = bf16[16,32,1,32,128]{4,3,1,2,0:T(8,128)(2,1)} all-to-all(bf16[16,32,1,32,128]{4,3,1,2,0:T(8,128)(2,1)S(1)} %bitcast.143), channel_id=1, replica_groups=mesh['sp'=32,'tp_0'=4,'tp_1'=4] {'tp_0','tp_1'}, dimensions={0} | all-to-all | bytes 8388608 | tf_op jit(solution)/shard_map/all_to_all | solution.py:38
  262.8 3.5 %reduce_sum.86 = bf16[32,32,128]{2,1,0:T(8,128)(2,1)} reduce(bf16[16,32,1,32,128]{4,3,1,2,0:T(8,128)(2,1)} %all_to_all.26, bf16[]{:T(256)} %constant.38.clone.1), dimensions={0,2}, to_apply=%region_15.16 | reduce | flops 1966080 | bytes 4456450 | tf_op jit(solution)/shard_map/reduce_sum | solution.py:39
  266.4 15.5 %all-to-all-start.4 = ((bf16[32,32,128]{2,1,0:T(8,128)(2,1)}), bf16[32,32,128]{2,1,0:T(8,128)(2,1)S(1)}, u32[]{:S(2)}, u32[]{:S(2)}) async-start(bf16[32,32,128]{2,1,0:T(8,128)(2,1)} %reduce_sum.86), calls=%async_computation.4 | async-start | bytes 524288 | tf_op jit(solution)/shard_map/all_to_all | solution.py:149
  281.9 0.1 mul.536
  282.0 0.1 copy.34
  282.2 22.0 %all-to-all-done.4 = bf16[32,32,128]{2,1,0:T(8,128)(2,1)S(1)} async-done(((bf16[32,32,128]{2,1,0:T(8,128)(2,1)}), bf16[32,32,128]{2,1,0:T(8,128)(2,1)S(1)}, u32[]{:S(2)}, u32[]{:S(2)}) %all-to-all-start.4) | async-done | bytes 262176 | tf_op jit(solution)/shard_map/all_to_all | solution.py:149
  304.2 1.9 gather_fusion
  306.0 0.3 fusion.19
  306.4 0.6 add_convert_fusion
  (27 shorter events, 0.2 us)
Async XLA Ops:
  6.5 189.7 %copy-start = (bf16[1,256,2048]{2,1,0:T(8,128)(2,1)S(1)}, bf16[1,256,2048]{2,1,0:T(8,128)(2,1)}, u32[]{:S(2)}) copy-start(bf16[1,256,2048]{2,1,0:T(8,128)(2,1)} %param.27) | copy-start | bytes 3145732
  6.5 31.9 %copy-start.6 = (s32[192,4]{0,1:T(4,128)S(1)}, s32[192,4]{0,1:T(4,128)}, u32[]{:S(2)}) copy-start(s32[192,4]{0,1:T(4,128)} %param.23) | copy-start | bytes 9220
  6.5 47.0 %copy-start.5 = (f32[2048]{0:T(1024)S(1)}, f32[2048]{0:T(1024)}, u32[]{:S(2)}) copy-start(f32[2048]{0:T(1024)} %param.20) | copy-start | bytes 24580
  7.5 8.8 %collective-permute-start = (bf16[30,128]{1,0:T(8,128)(2,1)S(1)}, bf16[30,128]{1,0:T(8,128)(2,1)S(1)}, u32[]{:S(2)}, u32[]{:S(2)}) collective-permute-start(bf16[30,128]{1,0:T(8,128)(2,1)S(1)} %slice.258), channel_id=1, source_target_pairs={{0,16},{16,32},{32,48},{48,64},{64,80},{80,96},{96,112},{112,128},... | collective-permute-start | bytes 23048 | tf_op jit(solution)/shard_map/ppermute | solution.py:21
  34.8 18.4 %all-to-all-start = ((bf16[16,12,2048]{2,1,0:T(8,128)(2,1)}), bf16[16,12,2048]{2,1,0:T(8,128)(2,1)S(1)}, u32[]{:S(2)}, u32[]{:S(2)}) async-start(bf16[16,12,2048]{2,1,0:T(8,128)(2,1)} %reshape.122), calls=%async_computation | async-start | bytes 2097152 | tf_op jit(solution)/shard_map/all_to_all | solution.py:38
  38.5 33.9 %copy-start.1 = (bf16[2048,128]{1,0:T(8,128)(2,1)S(1)}, bf16[2048,128]{1,0:T(8,128)(2,1)}, u32[]{:S(2)}) copy-start(bf16[2048,128]{1,0:T(8,128)(2,1)} %param.21) | copy-start | bytes 1572868
  38.5 33.9 %copy-start.2 = (bf16[192,128]{1,0:T(8,128)(2,1)S(1)}, bf16[192,128]{1,0:T(8,128)(2,1)}, u32[]{:S(2)}) copy-start(bf16[192,128]{1,0:T(8,128)(2,1)} %param.14) | copy-start | bytes 147460
  54.7 17.4 %all-to-all-start.1 = ((bf16[16,12,2048]{2,1,0:T(8,128)(2,1)}), bf16[16,12,2048]{2,1,0:T(8,128)(2,1)S(1)}, u32[]{:S(2)}, u32[]{:S(2)}) async-start(bf16[16,12,2048]{2,1,0:T(8,128)(2,1)} %broadcast_in_dim.2), calls=%async_computation.1 | async-start | bytes 2097152 | tf_op jit(solution)/shard_map/all_to_all | solution.py:44
  58.5 133.0 %all-gather.2.cloned.1.call-start = ((), (), s32[]{:S(2)}) async-start(), calls=%async_computation.5 | async-start | bytes 4456448 | tf_op jit(solution)/shard_map/all_gather | solution.py:123
  60.7 0.6 copy-start.3
  132.9 63.4 %copy-start.8 = (bf16[1,2048,256]{2,1,0:T(8,128)(2,1)S(1)}, bf16[1,2048,256]{2,1,0:T(8,128)(2,1)}, u32[]{:S(2)}) copy-start(bf16[1,2048,256]{2,1,0:T(8,128)(2,1)} %param.26) | copy-start | bytes 3145732
  262.8 19.2 %copy-start.7 = (f32[192,4]{0,1:T(4,128)S(1)}, f32[192,4]{0,1:T(4,128)}, u32[]{:S(2)}) copy-start(f32[192,4]{0,1:T(4,128)} %param.24) | copy-start | bytes 9220
  262.8 19.3 %copy-start.4 = (s32[768]{0:T(1024)S(1)}, s32[768]{0:T(1024)}, u32[]{:S(2)}) copy-start(s32[768]{0:T(1024)} %copy-done.3) | copy-start | bytes 9220
  266.4 37.8 %all-to-all-start.4 = ((bf16[32,32,128]{2,1,0:T(8,128)(2,1)}), bf16[32,32,128]{2,1,0:T(8,128)(2,1)S(1)}, u32[]{:S(2)}, u32[]{:S(2)}) async-start(bf16[32,32,128]{2,1,0:T(8,128)(2,1)} %reduce_sum.86), calls=%async_computation.4 | async-start | bytes 524288 | tf_op jit(solution)/shard_map/all_to_all | solution.py:149
Sparse Core Ops, SparseCore 0:
  133.0 58.3 all-gather.1
where the time goes:
time: 315 us; the launch traced here: 314 us
  blocking collectives  128 us (41%)
  waiting for transfers between devices  106 us (34%)
  starting transfers between devices  27.8 us (9%)
  matrix products  17 us (5%)
  between operations  13.7 us (4%)
  local copies, waits for them, and re-layouts  11.2 us (4%)
  other arithmetic  9.51 us (3%)
    all_gather x1, waiting for transfers between devices, shards(): lax.all_gather(lax.all_to_all(outgoing, 'sp', split_axis=0, concat_axis=0...  58.5 us
    all_to_all x1, blocking collectives, summed_on_arrival(): lax.all_to_all(pieces, axis, split_axis=0, concat_axis=0, tiled=True)  54.5 us
    all_to_all x1, blocking collectives, shards(): lax.all_to_all(outgoing, 'sp', split_axis=0, concat_axis=0, tiled=True)  44.7 us
    psum x4, blocking collectives, over_axes(): value = lax.psum(value, axis)  29.2 us
    all_to_all x1, waiting for transfers between devices, shards(): lax.all_to_all(summed.reshape(sources * local_experts, count, summed.shap...  22 us
    all_to_all x1, starting transfers between devices, shards(): lax.all_to_all(summed.reshape(sources * local_experts, count, summed.shap...  15.5 us
    all_to_all x1, waiting for transfers between devices, summed_on_arrival(): lax.all_to_all(pieces, axis, split_axis=0, concat_axis=0, tiled=True)  14.4 us
    all_to_all x1, waiting for transfers between devices, from_everyone(): return lax.all_to_all(copies, axis, split_axis=0, concat_axis=0, tiled=True)  9.49 us
  transfers between devices with their start and end apart: 5, of which 5 were waited for; matrix products, arithmetic and copies ran while one was open for 2% of the time, Pallas kernels for 0%

commit v1 on v0

--- a/solution.py
+++ b/solution.py
@@ -1,6 +1,8 @@
 import jax
 import jax.numpy as jnp
 from jax import lax
+from jax.experimental import pallas as pl
+from jax.experimental.pallas import tpu as pltpu
 from jax.sharding import Mesh
 from jax.sharding import PartitionSpec as P
 
@@ -8,11 +10,390 @@
 TOPK = 4
 CAP = 32
 TP = ("tp_0", "tp_1")
-
+MESH = pl.DeviceIdType.MESH
 
 epsilon = 1e-05
 clamp_limit = 7.0
 swish_slope = 1.702
+
+SIDE = 4
+CHIPS = 16
+LANES = 128
+ROWS = E * CAP
+CHUNKS = 4
+CROWS = ROWS // CHUNKS
+PERCHUNK = CROWS // CAP
+OFFSETS = [0, 1, -1, 2, -2, 3, -3, 4, -4, 5, -5, 6, -6, 7, -7, 8]
+
+
+class Plane:
+    def __init__(self, y, x):
+        self.pos = (y, x)
+        self.axes = ("tp_0", "tp_1")
+
+    def neighbour(self, dim, step):
+        return {self.axes[dim]: lax.rem(self.pos[dim] + step + SIDE, SIDE)}
+
+    def at(self, dim, step):
+        return lax.rem(self.pos[dim] + step + SIDE, SIDE)
+
+    def line(self, ref, dim, index, rows):
+        if dim == 0:
+            return ref.at[index, :, rows, :]
+        return ref.at[:, index, rows, :]
+
+    def one(self, ref, dim, index, rows):
+        if dim == 0:
+            return ref.at[index, self.pos[1], rows, :]
+        return ref.at[self.pos[0], index, rows, :]
+
+
+def copy_to(src, dst, send, recv, device):
+    return pltpu.make_async_remote_copy(
+        src_ref=src, dst_ref=dst, send_sem=send, recv_sem=recv, device_id=device, device_id_type=MESH
+    )
+
+
+class Gather:
+    def __init__(self, plane, buf, base, count, send, recv, chunk):
+        self.plane, self.buf, self.chunk = plane, buf, chunk
+        self.send, self.recv = send, recv
+        self.half = count // 2
+        self.quarter = count // 4
+        self.base = base
+        self.pending = {}
+
+    def rows(self, color):
+        start = self.base + color * self.half
+        return pl.ds(start, self.half)
+
+    def part(self, color, which):
+        start = self.base + color * self.half + which * self.quarter
+        return pl.ds(start, self.quarter)
+
+    def go(self, color, step, way, src, dst, device):
+        sem = (self.chunk, color, step, way)
+        op = copy_to(src, dst, self.send.at[sem], self.recv.at[sem], device)
+        op.start()
+        self.pending[(color, step, way)] = op
+
+    def issue(self, step):
+        plane = self.plane
+        for color in range(2):
+            near = 1 - color
+            far = color
+            dim = near if step < 2 else far
+            view = plane.one if step < 2 else plane.line
+            ahead, behind = plane.neighbour(dim, 1), plane.neighbour(dim, -1)
+            if step % 2 == 0:
+                block = view(self.buf, dim, plane.pos[dim], self.rows(color))
+                self.go(color, step, 0, block, block, ahead)
+                self.go(color, step, 1, block, block, behind)
+            else:
+                self.pending[(color, step - 1, 0)].wait_recv()
+                block = view(self.buf, dim, plane.at(dim, -1), self.part(color, 0))
+                self.go(color, step, 0, block, block, ahead)
+                self.pending[(color, step - 1, 1)].wait_recv()
+                block = view(self.buf, dim, plane.at(dim, 1), self.part(color, 1))
+                self.go(color, step, 1, block, block, behind)
+
+    def arrived(self, step):
+        for color in range(2):
+            for way in range(2):
+                self.pending[(color, step, way)].wait_recv()
+
+    def sent(self):
+        for op in self.pending.values():
+            op.wait_send()
+
+
+class Reduce:
+    def __init__(self, plane, buf, base, count, lands, send, recv, chunk):
+        self.plane, self.buf, self.chunk = plane, buf, chunk
+        self.send, self.recv = send, recv
+        self.half = count // 2
+        self.quarter = count // 4
+        self.base = base
+        self.lands = lands
+        self.pending = {}
+
+    def rows(self, color):
+        return pl.ds(self.base + color * self.half, self.half)
+
+    def part(self, color, which):
+        return pl.ds(self.base + color * self.half + which * self.quarter, self.quarter)
+
+    def go(self, color, step, way, src, device):
+        sem = (self.chunk, color, step, way)
+        dst = self.lands[step].at[self.chunk, color, way]
+        op = copy_to(src, dst, self.send.at[sem], self.recv.at[sem], device)
+        op.start()
+        self.pending[(color, step, way)] = op
+
+    def land(self, color, step, way):
+        self.pending[(color, step, way)].wait_recv()
+        return self.lands[step].at[self.chunk, color, way]
+
+    def issue(self, step):
+        plane = self.plane
+        for color in range(2):
+            near = 1 - color
+            far = color
+            dim = far if step < 2 else near
+            view = plane.line if step < 2 else plane.one
+            ahead, behind = plane.neighbour(dim, 1), plane.neighbour(dim, -1)
+            if step == 2:
+                self.fold(color)
+            if step % 2 == 0:
+                opposite = plane.at(dim, 2)
+                self.go(color, step, 0, view(self.buf, dim, opposite, self.part(color, 0)), ahead)
+                self.go(color, step, 1, view(self.buf, dim, opposite, self.part(color, 1)), behind)
+            else:
+                for way, (shift, device) in enumerate(((1, ahead), (-1, behind))):
+                    landed = self.land(color, step - 1, way)
+                    target = view(self.buf, dim, plane.at(dim, shift), self.part(color, way))
+                    target[...] = (target[...].astype(jnp.float32) + landed[...].astype(jnp.float32)).astype(
+                        jnp.bfloat16
+                    )
+                    whole = view(self.buf, dim, plane.at(dim, shift), self.rows(color))
+                    self.go(color, step, way, whole, device)
+
+    def fold(self, color):
+        plane = self.plane
+        far = color
+        own = plane.line(self.buf, far, plane.pos[far], self.rows(color))
+        first, second = self.land(color, 1, 0), self.land(color, 1, 1)
+        own[...] = (
+            own[...].astype(jnp.float32) + first[...].astype(jnp.float32) + second[...].astype(jnp.float32)
+        ).astype(jnp.bfloat16)
+
+    def total(self, color):
+        plane = self.plane
+        near = 1 - color
+        own = plane.one(self.buf, near, plane.pos[near], self.rows(color))
+        first, second = self.land(color, 3, 0), self.land(color, 3, 1)
+        return own[...].astype(jnp.float32) + first[...].astype(jnp.float32) + second[...].astype(jnp.float32)
+
+    def sent(self):
+        for op in self.pending.values():
+            op.wait_send()
+
+
+def land_shapes(chunks, count):
+    half, quarter = count // 2, count // 4
+    return [
+        pltpu.VMEM((chunks, 2, 2, SIDE, quarter, LANES), jnp.bfloat16),
+        pltpu.VMEM((chunks, 2, 2, SIDE, half, LANES), jnp.bfloat16),
+        pltpu.VMEM((chunks, 2, 2, quarter, LANES), jnp.bfloat16),
+        pltpu.VMEM((chunks, 2, 2, half, LANES), jnp.bfloat16),
+    ]
+
+
+def expert_kernel(
+    outgoing,
+    middle,
+    mix_hi,
+    mix_lo,
+    gain,
+    gate_hbm,
+    up_hbm,
+    down_hbm,
+    result,
+    gate,
+    up,
+    down,
+    rows,
+    normed,
+    partial,
+    land0,
+    land1,
+    land2,
+    land3,
+    total,
+    back,
+    weight_sem,
+    ag_send,
+    ag_recv,
+    rs_send,
+    rs_recv,
+    out_send,
+    out_recv,
+    back_send,
+    back_recv,
+):
+    sp = lax.axis_index("sp")
+    y, x = lax.axis_index("tp_0"), lax.axis_index("tp_1")
+    z, core = sp // 2, lax.rem(sp, 2)
+    plane = Plane(y, x)
+
+    barrier = pltpu.get_barrier_semaphore()
+
+    @pl.loop(1, E)
+    def _(d):
+        pl.semaphore_signal(barrier, inc=1, device_id={"sp": lax.rem(sp + d, E)}, device_id_type=MESH)
+
+    for dim in range(2):
+        for step in (1, -1):
+            pl.semaphore_signal(barrier, inc=1, device_id=plane.neighbour(dim, step), device_id_type=MESH)
+
+    fetches = [
+        pltpu.make_async_copy(src.at[0], dst, weight_sem.at[i])
+        for i, (src, dst) in enumerate(((gate_hbm, gate), (up_hbm, up), (down_hbm, down)))
+    ]
+    for fetch in fetches:
+        fetch.start()
+    pl.semaphore_wait(barrier, E - 1 + 4)
+
+    other = 1 - core
+    for i, offset in enumerate(OFFSETS):
+        chip = lax.rem(z - offset + CHIPS, CHIPS)
+        place = pl.ds(pl.multiple_of((2 * i + core) * CAP, CAP), CAP)
+        for way in range(2):
+            if i == 0 and way == 1:
+                continue
+            target = 2 * chip + (other if i == 0 else way)
+            copy_to(
+                outgoing.at[target],
+                rows.at[y, x, place, :],
+                out_send,
+                out_recv.at[2 * i // PERCHUNK],
+                {"sp": target},
+            ).start()
+    own_place = pl.ds(pl.multiple_of(core * CAP, CAP), CAP)
+    rows[y, x, own_place, :] = outgoing[sp]
+
+    gathers = [Gather(plane, rows, c * CROWS, CROWS, ag_send, ag_recv, c) for c in range(CHUNKS)]
+    lands = (land0, land1, land2, land3)
+    reduces = [Reduce(plane, partial, c * CROWS, CROWS, lands, rs_send, rs_recv, c) for c in range(CHUNKS)]
+
+    def begin(c):
+        count = CROWS - (CAP if c == 0 else 0)
+        landed = rows.at[y, x, pl.ds(c * CROWS, count), :]
+        copy_to(landed, landed, out_send, out_recv.at[c], {"sp": sp}).wait_recv()
+        gathers[c].issue(0)
+
+    def compute(c):
+        gathers[c].arrived(3)
+        if c == 0:
+            for fetch in fetches:
+                fetch.wait()
+        step = 32
+
+        @pl.loop(0, CROWS // step)
+        def _(i):
+            at = pl.multiple_of(i * step, step)
+            block = rows[:, :, pl.ds(c * CROWS + at, step), :].astype(jnp.float32)
+            block = block.reshape(SIDE * SIDE, step, LANES)
+            squares = jnp.sum(jnp.sum(block * block, axis=0), axis=1, keepdims=True)
+            scale = lax.rsqrt(squares / (SIDE * SIDE * LANES) + epsilon)
+            scaled = block * scale[None] * gain[...][:, None, :]
+            normed[:, pl.ds(at, step), :] = scaled.astype(jnp.bfloat16)
+
+        left = jnp.concatenate([normed[b] for b in range(SIDE * SIDE)], axis=1)
+        gate_pre = jnp.minimum(jnp.dot(left, gate[...], preferred_element_type=jnp.float32), clamp_limit)
+        up_pre = jnp.clip(
+            jnp.dot(left, up[...], preferred_element_type=jnp.float32), -clamp_limit, clamp_limit
+        )
+        hidden = (gate_pre * jax.nn.sigmoid(swish_slope * gate_pre) * (up_pre + 1.0)).astype(jnp.bfloat16)
+        place = pl.ds(c * CROWS, CROWS)
+        for j in range(SIDE * SIDE // 2):
+            both = jnp.dot(
+                hidden, down[:, 2 * j * LANES : 2 * (j + 1) * LANES], preferred_element_type=jnp.float32
+            ).astype(jnp.bfloat16)
+            for k in range(2):
+                b = 2 * j + k
+                partial[b // SIDE, b % SIDE, place, :] = both[:, k * LANES : (k + 1) * LANES]
+        reduces[c].issue(0)
+
+    def finish(c):
+        half = CROWS // 2
+        for color in range(2):
+            total[pl.ds(c * CROWS + color * half, half), :] = reduces[c].total(color).astype(jnp.bfloat16)
+        for p in range(c * PERCHUNK, (c + 1) * PERCHUNK):
+            i, way = p // 2, p % 2
+            if i == 0 and way == 1:
+                continue
+            chip = lax.rem(z + OFFSETS[i] + CHIPS, CHIPS)
+            if i == 0:
+                target = 2 * chip + other
+                src = total.at[pl.ds(pl.multiple_of(other * CAP, CAP), CAP), :]
+            else:
+                target = 2 * chip + way
+                src = total.at[pl.ds(p * CAP, CAP), :]
+            copy_to(src, back.at[sp], back_send, back_recv, {"sp": target}).start()
+        if c == 0:
+            back[sp] = total[own_place, :]
+
+    stages = [
+        begin,
+        lambda c: gathers[c].issue(1),
+        lambda c: (gathers[c].arrived(1), gathers[c].issue(2)),
+        lambda c: gathers[c].issue(3),
+        compute,
+        lambda c: reduces[c].issue(1),
+        lambda c: reduces[c].issue(2),
+        lambda c: reduces[c].issue(3),
+        finish,
+    ]
+    for slot in range(CHUNKS + len(stages) - 1):
+        for stage in (0, 1, 2, 3, 5, 6, 7, 8, 4):
+            c = slot - stage
+            if 0 <= c < CHUNKS:
+                stages[stage](c)
+
+    whole = back.at[pl.ds(0, E - 1)]
+    copy_to(whole, whole, back_send, back_recv, {"sp": sp}).wait_recv()
+    values = back[...].reshape(ROWS, LANES)
+    routed = jnp.dot(mix_hi[...], values, preferred_element_type=jnp.float32)
+    routed = routed + jnp.dot(mix_lo[...], values, preferred_element_type=jnp.float32)
+    result[...] = (middle[...].astype(jnp.float32) + routed).astype(jnp.bfloat16)
+
+    sent = outgoing.at[pl.ds(0, E - 1)]
+    copy_to(sent, sent, out_send, out_recv.at[0], {"sp": sp}).wait_send()
+    sent = total.at[pl.ds(0, ROWS - CAP), :]
+    copy_to(sent, sent, back_send, back_recv, {"sp": sp}).wait_send()
+    for c in range(CHUNKS):
+        gathers[c].sent()
+        reduces[c].sent()
+
+
+def experts(outgoing, middle, mix_hi, mix_lo, gain, gate_experts, up_experts, down_experts):
+    vmem = pl.BlockSpec(memory_space=pltpu.VMEM)
+    hbm = pl.BlockSpec(memory_space=pl.ANY)
+    bf16 = jnp.bfloat16
+    depth, hidden = gate_experts.shape[1], gate_experts.shape[2]
+    sems = pltpu.SemaphoreType.DMA((CHUNKS, 2, 4, 2))
+    one = pltpu.SemaphoreType.DMA
+    return pl.pallas_call(
+        expert_kernel,
+        out_shape=jax.ShapeDtypeStruct(middle.shape, bf16),
+        in_specs=[vmem] * 5 + [hbm] * 3,
+        out_specs=vmem,
+        scratch_shapes=[
+            pltpu.VMEM((depth, hidden), bf16),
+            pltpu.VMEM((depth, hidden), bf16),
+            pltpu.VMEM((hidden, depth), bf16),
+            pltpu.VMEM((SIDE, SIDE, ROWS, LANES), bf16),
+            pltpu.VMEM((SIDE * SIDE, CROWS, LANES), bf16),
+            pltpu.VMEM((SIDE, SIDE, ROWS, LANES), bf16),
+            *land_shapes(CHUNKS, CROWS),
+            pltpu.VMEM((ROWS, LANES), bf16),
+            pltpu.VMEM((E, CAP, LANES), bf16),
+            one((3,)),
+            sems,
+            sems,
+            sems,
+            sems,
+            one,
+            one((CHUNKS,)),
+            one,
+            one,
+        ],
+        compiler_params=pltpu.CompilerParams(
+            collective_id=1, has_side_effects=True, vmem_limit_bytes=48 * 1024 * 1024
+        ),
+        name="experts",
+    )(outgoing, middle, mix_hi, mix_lo, gain, gate_experts, up_experts, down_experts)
 
 
 def from_behind(block, axis, distance):
@@ -100,63 +481,27 @@
     ).astype(jnp.bfloat16)
     branch = jnp.dot(gathered_copies(mixed, TP, 0), out_weight, preferred_element_type=jnp.float32)
     middle = (resid.astype(jnp.float32) + branch).astype(jnp.bfloat16)
-    middle32 = middle.astype(jnp.float32)
-    feat_total = feat_local * lax.axis_size(TP)
-    squares = over_axes(jnp.sum(middle32 * middle32, axis=1), TP)
-    normed = (middle32 * lax.rsqrt(squares[:, None] / feat_total + epsilon) * norm_gain).astype(
-        jnp.bfloat16
-    )
+    gain = from_everyone(norm_gain, TP).reshape(SIDE * SIDE, LANES)
+
     flat_ids = route_ids.reshape(-1)
     expert_table = (flat_ids[:, None] == jnp.arange(E, dtype=jnp.int32)[None, :]).astype(jnp.int32)
     earlier_count = jnp.cumsum(expert_table, axis=0) - expert_table
     position = jnp.sum(earlier_count * expert_table, axis=1)
-    slot_of = flat_ids * CAP + position
-    slot_grid = slot_of.reshape(tok_rows, TOPK)
-    picker = jnp.any(
-        slot_grid[None, :, :] == jnp.arange(E * CAP, dtype=jnp.int32)[:, None, None], axis=2
-    ).astype(jnp.bfloat16)
+    slot_grid = (flat_ids * CAP + position).reshape(tok_rows, TOPK)
+    hits = slot_grid[None, :, :] == jnp.arange(E * CAP, dtype=jnp.int32)[:, None, None]
+    picker = jnp.any(hits, axis=2).astype(jnp.bfloat16)
     outgoing = (
-        jnp.dot(picker, normed, preferred_element_type=jnp.float32)
+        jnp.dot(picker, middle, preferred_element_type=jnp.float32)
         .astype(jnp.bfloat16)
         .reshape(E, CAP, feat_local)
     )
-    received = lax.all_gather(
-        lax.all_to_all(outgoing, "sp", split_axis=0, concat_axis=0, tiled=True),
-        TP,
-        axis=2,
-        tiled=True,
-    )
-    local_experts = gate_experts.shape[0]
-    sources = received.shape[0] // local_experts
-    count = received.shape[1]
-    rows = received.reshape(sources, local_experts, count, received.shape[2])
-    gate_pre = jnp.minimum(
-        jnp.einsum("sjcd,jdf->sjcf", rows, gate_experts, preferred_element_type=jnp.float32),
-        clamp_limit,
-    )
-    up_pre = jnp.clip(
-        jnp.einsum("sjcd,jdf->sjcf", rows, up_experts, preferred_element_type=jnp.float32),
-        -clamp_limit,
-        clamp_limit,
-    )
-    hidden = (gate_pre * jax.nn.sigmoid(swish_slope * gate_pre) * (up_pre + 1.0)).astype(
-        jnp.bfloat16
-    )
-    partial_value = jnp.einsum(
-        "sjcf,jfd->sjcd", hidden, down_experts, preferred_element_type=jnp.float32
-    )
-    summed = summed_on_arrival(partial_value.astype(jnp.bfloat16), TP, 3).astype(jnp.bfloat16)
-    returned = lax.all_to_all(
-        summed.reshape(sources * local_experts, count, summed.shape[3]),
-        "sp",
-        split_axis=0,
-        concat_axis=0,
-        tiled=True,
-    )
-    flat_back = returned.reshape(E * CAP, feat_local)
-    picked = flat_back[slot_of].astype(jnp.float32).reshape(tok_rows, TOPK, feat_local)
-    routed_sum = jnp.sum(picked * route_weights[:, :, None], axis=1)
-    return (middle32 + routed_sum).astype(jnp.bfloat16)
+    back_hits = slot_grid[:, :, None] == jnp.arange(E * CAP, dtype=jnp.int32)[None, None, :]
+    mixer = jnp.sum(jnp.where(back_hits, route_weights[:, :, None], 0.0), axis=1)
+    mix_hi = lax.reduce_precision(mixer, 8, 7)
+    mix_lo = (mixer - mix_hi).astype(jnp.bfloat16)
+    return experts(
+        outgoing, middle, mix_hi.astype(jnp.bfloat16), mix_lo, gain, gate_experts, up_experts, down_experts
+    )
 
 
 def solution(mesh):

time: 315 us -> 177 us (0.56)
  blocking collectives: 128 us -> 15.3 us
  Pallas kernels: 0 us -> 97.7 us
  waiting for transfers between devices: 106 us -> 28.2 us
  between operations: 13.7 us -> 0.21 us
  matrix products: 17 us -> 4.04 us
  starting transfers between devices: 27.8 us -> 16.4 us
  other arithmetic: 9.51 us -> 5.45 us
    all_to_all x2 -> x0, blocking collectives: 99.1 us -> none  [the longest x1 54.5 us: summed_on_arrival(): lax.all_to_all(pieces, axis, split_axis=0, concat_axis=0, tiled=True)]
    pallas_call x0 -> x1, Pallas kernels: none -> 97.7 us  [experts(): pl.pallas_call(expert_kernel, out_shape=jax.ShapeDtypeStruct(middle.shape...]
    all_gather x1 -> x0, waiting for transfers between devices: 58.5 us -> none  [shards(): lax.all_gather(lax.all_to_all(outgoing, 'sp', split_axis=0, concat_axis=0...]
    all_to_all x1 -> x0, waiting for transfers between devices: 22 us -> none  [shards(): lax.all_to_all(summed.reshape(sources * local_experts, count, summed.shap...]
    all_to_all x1 -> x0, starting transfers between devices: 15.5 us -> none  [shards(): lax.all_to_all(summed.reshape(sources * local_experts, count, summed.shap...]
    psum x4 -> x2, blocking collectives: 29.2 us -> 15.3 us  [over_axes(): value = lax.psum(value, axis)]
    dot_general x3 -> x1, matrix products: 15.1 us -> 1.22 us  [shards(): jnp.dot(picker, middle, preferred_element_type=jnp.float32)]
    all_to_all x1 -> x2, waiting for transfers between devices: 9.49 us -> 14.3 us  [from_everyone(): return lax.all_to_all(copies, axis, split_axis=0, concat_axis=0, tiled=True)]
  transfers between devices with their start and end apart: 5 -> 4, of which waited for: 5 -> 4; matrix products, arithmetic and copies ran while one was open for 2% -> 6% of each run, Pallas kernels for 0% -> 0%
where the time goes in v1:
time: 177 us
  Pallas kernels  97.7 us (55%)
  waiting for transfers between devices  28.2 us (16%)
  starting transfers between devices  16.4 us (9%)
  blocking collectives  15.3 us (9%)
  local copies, waits for them, and re-layouts  9.52 us (5%)
  other arithmetic  5.45 us (3%)
  matrix products  4.04 us (2%)
    pallas_call x1, Pallas kernels, experts(): pl.pallas_call(expert_kernel, out_shape=jax.ShapeDtypeStruct(middle.shape...  97.7 us
    psum x2, blocking collectives, over_axes(): value = lax.psum(value, axis)  15.3 us
    all_to_all x2, waiting for transfers between devices, from_everyone(): return lax.all_to_all(copies, axis, split_axis=0, concat_axis=0, tiled=True)  14.3 us
    all_to_all x1, waiting for transfers between devices, summed_on_arrival(): lax.all_to_all(pieces, axis, split_axis=0, concat_axis=0, tiled=True)  12 us
    all_to_all x2, starting transfers between devices, from_everyone(): return lax.all_to_all(copies, axis, split_axis=0, concat_axis=0, tiled=True)  7.68 us
    ppermute x1, starting transfers between devices, from_behind(): return lax.ppermute(block, axis, route)  4.92 us
    all_to_all x1, starting transfers between devices, summed_on_arrival(): lax.all_to_all(pieces, axis, split_axis=0, concat_axis=0, tiled=True)  3.78 us
  transfers between devices with their start and end apart: 4, of which 4 were waited for; matrix products, arithmetic and copies ran while one was open for 6% of the time, Pallas kernels for 0%

profile of v1, /device:TPU:1, one launch (start us, length us, event | category | flops | bytes accessed | tf_op | source)
XLA Modules:
  0.0 176.8 jit_solution(10349344510227426383)
XLA Ops:
  0.0 0.0 copy-start
  0.0 0.9 multiply_convert_fusion.2
  0.9 4.9 %collective-permute-start = (bf16[30,128]{1,0:T(8,128)(2,1)S(1)}, bf16[30,128]{1,0:T(8,128)(2,1)S(1)}, u32[]{:S(2)}, u32[]{:S(2)}) collective-permute-start(bf16[30,128]{1,0:T(8,128)(2,1)S(1)} %slice.257), channel_id=1, source_target_pairs={{0,16},{16,32},{32,48},{48,64},{64,80},{80,96},{96,112},{112,128},... | collective-permute-start | bytes 23048 | tf_op jit(solution)/shard_map/ppermute | solution.py:402
  5.9 1.0 slice_bitcast_fusion.30
  6.9 1.0 slice_bitcast_fusion.29
  7.8 1.9 %collective-permute-done = bf16[30,128]{1,0:T(8,128)(2,1)S(1)} collective-permute-done((bf16[30,128]{1,0:T(8,128)(2,1)S(1)}, bf16[30,128]{1,0:T(8,128)(2,1)S(1)}, u32[]{:S(2)}, u32[]{:S(2)}) %collective-permute-start) | collective-permute-done | bytes 7712 | tf_op jit(solution)/shard_map/ppermute | solution.py:402
  9.7 0.5 fusion.41
  10.2 7.1 %all-reduce.1 = (f32[192]{0:T(256)S(1)}, f32[192]{0:T(256)S(1)}) all-reduce(f32[192]{0:T(256)S(1)} %get-tuple-element.6, f32[192]{0:T(256)S(1)} %get-tuple-element.5), channel_id=1, replica_groups=mesh['sp'=32,'tp_0'=4,'tp_1'=4] {'tp_0'}, use_global_device_ids=true, to_apply=%region_8.9 | all-reduce | flops 384 | bytes 3072 | tf_op jit(solution)/shard_map/psum | solution.py:407
  17.3 8.2 %all-reduce = (f32[192]{0:T(256)S(1)}, f32[192]{0:T(256)S(1)}) all-reduce(f32[192]{0:T(256)S(1)} %get-tuple-element.9, f32[192]{0:T(256)S(1)} %get-tuple-element.10), channel_id=1, replica_groups=mesh['sp'=32,'tp_0'=4,'tp_1'=4] {'tp_1'}, use_global_device_ids=true, to_apply=%region_9.10 | all-reduce | flops 384 | bytes 3072 | tf_op jit(solution)/shard_map/psum | solution.py:407
  25.6 0.0 copy-done
  25.6 1.1 convolution_convert_fusion
  26.7 1.2 reshape.59
  27.8 3.8 %all-to-all-start = ((bf16[16,12,2048]{2,1,0:T(8,128)(2,1)}), bf16[16,12,2048]{2,1,0:T(8,128)(2,1)S(1)}, u32[]{:S(2)}, u32[]{:S(2)}) async-start(bf16[16,12,2048]{2,1,0:T(8,128)(2,1)} %reshape.59), calls=%async_computation | async-start | bytes 2097152 | tf_op jit(solution)/shard_map/all_to_all | solution.py:419
  31.6 0.0 copy-done.7
  31.6 0.1 copy.37
  31.8 0.1 eq.55
  31.9 0.0 copy-start.8
  31.9 0.1 eq.51
  32.0 1.7 reduce-window.6
  33.8 0.3 slice_reduce_fusion
  34.1 0.1 fusion.5
  34.2 0.1 reduce_sum.57
  34.3 0.1 copy.40
  34.4 12.0 %all-to-all-done = bf16[16,12,2048]{2,1,0:T(8,128)(2,1)S(1)} async-done(((bf16[16,12,2048]{2,1,0:T(8,128)(2,1)}), bf16[16,12,2048]{2,1,0:T(8,128)(2,1)S(1)}, u32[]{:S(2)}, u32[]{:S(2)}) %all-to-all-start) | async-done | bytes 786464 | tf_op jit(solution)/shard_map/all_to_all | solution.py:419
  46.4 0.2 convert_reduce_fusion
  46.6 0.1 multiply_reduce_fusion
  46.7 0.0 copy-done.8
  46.7 0.1 multiply_convert_fusion
  46.8 1.1 broadcast_in_dim.12
  47.9 3.8 %all-to-all-start.1 = ((bf16[16,12,2048]{2,1,0:T(8,128)(2,1)}), bf16[16,12,2048]{2,1,0:T(8,128)(2,1)S(1)}, u32[]{:S(2)}, u32[]{:S(2)}) async-start(bf16[16,12,2048]{2,1,0:T(8,128)(2,1)} %broadcast_in_dim.12), calls=%async_computation.1 | async-start | bytes 2097152 | tf_op jit(solution)/shard_map/all_to_all | solution.py:425
  51.8 1.2 fusion
  53.0 0.0 copy-done.9
  53.0 0.4 select_reduce_fusion
  53.4 0.1 fusion.2
  53.5 0.0 copy-start.6
  53.5 12.0 %all-to-all-done.1 = bf16[16,12,2048]{2,1,0:T(8,128)(2,1)S(1)} async-done(((bf16[16,12,2048]{2,1,0:T(8,128)(2,1)}), bf16[16,12,2048]{2,1,0:T(8,128)(2,1)S(1)}, u32[]{:S(2)}, u32[]{:S(2)}) %all-to-all-start.1) | async-done | bytes 786464 | tf_op jit(solution)/shard_map/all_to_all | solution.py:425
  65.5 0.0 copy-done.10
  65.5 0.6 broadcast_in_dim.30
  66.1 3.8 %all-to-all-start.2 = ((f32[16,1,128]{2,1,0:T(1,128)}), f32[16,1,128]{2,1,0:T(1,128)S(1)}, u32[]{:S(2)}, u32[]{:S(2)}) async-start(f32[16,1,128]{2,1,0:T(1,128)} %broadcast_in_dim.30), calls=%async_computation.2 | async-start | bytes 16384 | tf_op jit(solution)/shard_map/all_to_all | solution.py:425
  69.9 0.0 copy-start.2
  69.9 1.1 reshape.60
  71.0 1.7 fusion.1.middle
  72.8 1.2 convolution_convert_fusion.1
  74.0 2.3 %all-to-all-done.2 = f32[16,1,128]{2,1,0:T(1,128)S(1)} async-done(((f32[16,1,128]{2,1,0:T(1,128)}), f32[16,1,128]{2,1,0:T(1,128)S(1)}, u32[]{:S(2)}, u32[]{:S(2)}) %all-to-all-start.2) | async-done | bytes 8224 | tf_op jit(solution)/shard_map/all_to_all | solution.py:425
  76.3 1.2 copy-done.3
  77.5 0.9 copy-done.4
  78.5 97.7 %experts.1 = bf16[192,128]{1,0:T(8,128)(2,1)S(1)} custom-call(bf16[32,32,128]{2,1,0:T(8,128)(2,1)S(1)} %bitcast.89, bf16[192,128]{1,0:T(8,128)(2,1)S(1)} %fusion.1.middle, bf16[192,1024]{1,0:T(8,128)(2,1)S(1)} %get-tuple-element.13.mix_hi, bf16[192,1024]{1,0:T(8,128)(2,1)S(1)} %get-tuple-element.12.mix_lo, f32[16,128]{1,0:T(8,128)S(1)} %bitcast.90, ...), custom_call_target="tpu_custom_call" | custom-call | tf_op jit(solution)/shard_map/experts/pallas_call | solution.py:367
  176.2 0.6 copy.44
  (17 shorter events, 0.1 us)
Async XLA Ops:
  0.0 25.6 %copy-start = (bf16[128,2048]{1,0:T(8,128)(2,1)S(1)}, bf16[128,2048]{1,0:T(8,128)(2,1)}, u32[]{:S(2)}) copy-start(bf16[128,2048]{1,0:T(8,128)(2,1)} %param.19) | copy-start | bytes 1572868
  0.9 8.8 %collective-permute-start = (bf16[30,128]{1,0:T(8,128)(2,1)S(1)}, bf16[30,128]{1,0:T(8,128)(2,1)S(1)}, u32[]{:S(2)}, u32[]{:S(2)}) collective-permute-start(bf16[30,128]{1,0:T(8,128)(2,1)S(1)} %slice.257), channel_id=1, source_target_pairs={{0,16},{16,32},{32,48},{48,64},{64,80},{80,96},{96,112},{112,128},... | collective-permute-start | bytes 23048 | tf_op jit(solution)/shard_map/ppermute | solution.py:402
  27.8 3.8 %copy-start.7 = (s32[192,4]{0,1:T(4,128)S(1)}, s32[192,4]{0,1:T(4,128)}, u32[]{:S(2)}) copy-start(s32[192,4]{0,1:T(4,128)} %param.23) | copy-start | bytes 9220
  27.8 18.5 %all-to-all-start = ((bf16[16,12,2048]{2,1,0:T(8,128)(2,1)}), bf16[16,12,2048]{2,1,0:T(8,128)(2,1)S(1)}, u32[]{:S(2)}, u32[]{:S(2)}) async-start(bf16[16,12,2048]{2,1,0:T(8,128)(2,1)} %reshape.59), calls=%async_computation | async-start | bytes 2097152 | tf_op jit(solution)/shard_map/all_to_all | solution.py:419
  31.9 14.8 %copy-start.8 = (f32[2048]{0:T(1024)S(1)}, f32[2048]{0:T(1024)}, u32[]{:S(2)}) copy-start(f32[2048]{0:T(1024)} %param.20) | copy-start | bytes 24580
  47.9 5.1 %copy-start.9 = (f32[192,4]{0,1:T(4,128)S(1)}, f32[192,4]{0,1:T(4,128)}, u32[]{:S(2)}) copy-start(f32[192,4]{0,1:T(4,128)} %param.24) | copy-start | bytes 9220
  47.9 17.6 %all-to-all-start.1 = ((bf16[16,12,2048]{2,1,0:T(8,128)(2,1)}), bf16[16,12,2048]{2,1,0:T(8,128)(2,1)S(1)}, u32[]{:S(2)}, u32[]{:S(2)}) async-start(bf16[16,12,2048]{2,1,0:T(8,128)(2,1)} %broadcast_in_dim.12), calls=%async_computation.1 | async-start | bytes 2097152 | tf_op jit(solution)/shard_map/all_to_all | solution.py:425
  53.0 12.5 %copy-start.10 = (f32[128]{0:T(128)S(1)}, f32[128]{0:T(128)}, u32[]{:S(2)}) copy-start(f32[128]{0:T(128)} %param.22) | copy-start | bytes 1540
  53.5 17.5 %copy-start.6 = (bf16[192,128]{1,0:T(8,128)(2,1)S(1)}, bf16[192,128]{1,0:T(8,128)(2,1)}, u32[]{:S(2)}) copy-start(bf16[192,128]{1,0:T(8,128)(2,1)} %param.14) | copy-start | bytes 147460
  66.1 10.2 %all-to-all-start.2 = ((f32[16,1,128]{2,1,0:T(1,128)}), f32[16,1,128]{2,1,0:T(1,128)S(1)}, u32[]{:S(2)}, u32[]{:S(2)}) async-start(f32[16,1,128]{2,1,0:T(1,128)} %broadcast_in_dim.30), calls=%async_computation.2 | async-start | bytes 16384 | tf_op jit(solution)/shard_map/all_to_all | solution.py:425
  69.9 6.4 %copy-start.2 = (bf16[1,2048,256]{2,1,0:T(8,128)(2,1)S(1)}, bf16[1,2048,256]{2,1,0:T(8,128)(2,1)}, u32[]{:S(2)}) copy-start(bf16[1,2048,256]{2,1,0:T(8,128)(2,1)} %up_hbm.1) | copy-start | bytes 3145732
  71.0 1.7 copy-start.5
  71.0 5.3 %copy-start.1 = (bf16[1,2048,256]{2,1,0:T(8,128)(2,1)S(1)}, bf16[1,2048,256]{2,1,0:T(8,128)(2,1)}, u32[]{:S(2)}) copy-start(bf16[1,2048,256]{2,1,0:T(8,128)(2,1)} %gate_hbm.1) | copy-start | bytes 3145732
  76.3 1.2 copy-start.3
  77.5 0.9 copy-start.4

commit v2 on v1

--- a/solution.py
+++ b/solution.py
@@ -179,6 +179,14 @@
             op.wait_send()
 
 
+MIX_CHUNKS = 1
+TOK = 192
+HALO = 32
+PAD_TOK = 256
+TAPS = 31
+WIDE = SIDE * SIDE * LANES
+
+
 def land_shapes(chunks, count):
     half, quarter = count // 2, count // 4
     return [
@@ -189,19 +197,52 @@
     ]
 
 
-def expert_kernel(
-    outgoing,
-    middle,
-    mix_hi,
-    mix_lo,
-    gain,
+def iota(shape, dim):
+    return lax.broadcasted_iota(jnp.int32, shape, dim)
+
+
+def layer_kernel(
+    value_hbm,
+    gating_hbm,
+    taps_hbm,
+    resid_hbm,
+    point_hbm,
+    outw_hbm,
     gate_hbm,
     up_hbm,
     down_hbm,
+    chan_gain,
+    mix_gain,
+    norm_gain,
+    routes,
     result,
+    value,
+    gating,
+    taps,
+    resid,
+    pointw,
+    outw,
     gate,
     up,
     down,
+    padded,
+    halo,
+    conv,
+    message,
+    stats,
+    gains,
+    scaled_out,
+    picker,
+    mixer_hi,
+    mixer_lo,
+    mid,
+    outgoing,
+    mix_part,
+    mix_rows,
+    mland0,
+    mland1,
+    mland2,
+    mland3,
     rows,
     normed,
     partial,
@@ -211,7 +252,15 @@
     land3,
     total,
     back,
-    weight_sem,
+    fetch_sem,
+    halo_send,
+    halo_recv,
+    stat_send,
+    stat_recv,
+    mag_send,
+    mag_recv,
+    mrs_send,
+    mrs_recv,
     ag_send,
     ag_recv,
     rs_send,
@@ -221,6 +270,7 @@
     back_send,
     back_recv,
 ):
+    f32, bf16 = jnp.float32, jnp.bfloat16
     sp = lax.axis_index("sp")
     y, x = lax.axis_index("tp_0"), lax.axis_index("tp_1")
     z, core = sp // 2, lax.rem(sp, 2)
@@ -232,29 +282,172 @@
     def _(d):
         pl.semaphore_signal(barrier, inc=1, device_id={"sp": lax.rem(sp + d, E)}, device_id_type=MESH)
 
-    for dim in range(2):
-        for step in (1, -1):
-            pl.semaphore_signal(barrier, inc=1, device_id=plane.neighbour(dim, step), device_id_type=MESH)
-
-    fetches = [
-        pltpu.make_async_copy(src.at[0], dst, weight_sem.at[i])
-        for i, (src, dst) in enumerate(((gate_hbm, gate), (up_hbm, up), (down_hbm, down)))
-    ]
-    for fetch in fetches:
+    mates = []
+    for dy in range(SIDE):
+        for dx in range(SIDE):
+            if dy or dx:
+                mates.append({"tp_0": lax.rem(y + dy, SIDE), "tp_1": lax.rem(x + dx, SIDE)})
+    for mate in mates:
+        pl.semaphore_signal(barrier, inc=1, device_id=mate, device_id_type=MESH)
+
+    fetches = []
+    for i, (src, dst) in enumerate(
+        (
+            (value_hbm, value),
+            (gating_hbm, gating),
+            (taps_hbm, taps),
+            (point_hbm, pointw),
+            (outw_hbm, outw),
+            (resid_hbm, resid),
+            (gate_hbm.at[0], gate),
+            (up_hbm.at[0], up),
+            (down_hbm.at[0], down),
+        )
+    ):
+        fetch = pltpu.make_async_copy(src, dst, fetch_sem.at[i])
         fetch.start()
-    pl.semaphore_wait(barrier, E - 1 + 4)
+        fetches.append(fetch)
+
+    for i in range(3):
+        fetches[i].wait()
+    unit = value[...].astype(f32) * jax.nn.sigmoid(gating[...].astype(f32))
+    padded[HALO:, :] = unit.astype(bf16).astype(f32)
+
+    def convolve(first, count):
+        acc = jnp.zeros((count, LANES), f32)
+        for tap in range(TAPS):
+            start = first + HALO - (TAPS - 1) + tap
+            acc = acc + padded[start : start + count, :] * taps[tap : tap + 1, :]
+        return acc
+
+    conv[HALO:, :] = convolve(HALO, TOK - HALO)
+
+    packed = routes[...]
+    turned = jnp.concatenate([packed, jnp.zeros((LANES - 8, PAD_TOK), f32)], axis=0).T
+    lanes_e = iota((TOK, E), 1).astype(f32)
+    member = jnp.zeros((TOK, E), f32)
+    weight = jnp.zeros((TOK, E), f32)
+    for k in range(TOPK):
+        hit = turned[:TOK, k : k + 1] == lanes_e
+        member = jnp.where(hit, 1.0, member)
+        weight = jnp.where(hit, turned[:TOK, TOPK + k : TOPK + k + 1], weight)
+    before = (iota((TOK, TOK), 1) < iota((TOK, TOK), 0)).astype(f32).astype(bf16)
+    place = jnp.dot(before, member.astype(bf16), preferred_element_type=f32)
+    place = jnp.where(member > 0.0, place, -1.0).astype(bf16)
+    weight_hi = weight.astype(bf16)
+    weight_lo = (weight - weight_hi.astype(f32)).astype(bf16)
+    for g in range(ROWS // LANES):
+        spread_to = (iota((E, LANES), 1) // CAP + g * (LANES // CAP) == iota((E, LANES), 0)).astype(f32).astype(bf16)
+        slots = jnp.dot(place, spread_to, preferred_element_type=f32)
+        mine = slots == lax.rem(iota((TOK, LANES), 1), CAP).astype(f32)
+        for part, held in ((weight_hi, mixer_hi), (weight_lo, mixer_lo)):
+            wide = jnp.dot(part, spread_to, preferred_element_type=f32)
+            held[:, g * LANES : (g + 1) * LANES] = jnp.where(mine, wide, 0.0).astype(bf16)
+
+    tall_e = iota((E, TOK), 0).astype(f32)
+    member = jnp.zeros((E, TOK), f32)
+    for k in range(TOPK):
+        member = jnp.where(packed[k : k + 1, :TOK] == tall_e, 1.0, member)
+    after = (iota((TOK, TOK), 0) < iota((TOK, TOK), 1)).astype(f32).astype(bf16)
+    place = jnp.dot(member.astype(bf16), after, preferred_element_type=f32)
+    place = jnp.where(member > 0.0, place, -1.0)
+    tall_c = iota((CAP, TOK), 0).astype(f32)
+    for e in range(E):
+        picker[e * CAP : (e + 1) * CAP, :] = (place[e : e + 1, :] == tall_c).astype(f32).astype(bf16)
+
+    fetches[4].wait()
+    columns = jnp.concatenate([mix_gain[...], jnp.zeros((LANES - SIDE * SIDE, LANES), f32)], axis=0).T
+    for b in range(SIDE * SIDE):
+        part = slice(b * LANES, (b + 1) * LANES)
+        scaled_out[part, :] = (outw[part, :].astype(f32) * columns[:, b : b + 1]).astype(bf16)
+
+    pl.semaphore_wait(barrier, E - 1 + len(mates))
+
+    tail = copy_to(padded.at[pl.ds(TOK, HALO), :], halo, halo_send, halo_recv, {"sp": lax.rem(sp + 1, E)})
+    tail.start()
+    tail.wait()
+    padded[:HALO, :] = jnp.where(sp > 0, halo[...], 0.0)
+    conv[:HALO, :] = convolve(0, HALO)
+
+    mean = jnp.mean(conv[...], axis=1, keepdims=True)
+    centred = conv[...] - mean
+    spread = jnp.sum(centred * centred, axis=1, keepdims=True)
+    lane = iota((TOK, LANES), 1)
+    both = jnp.where(lane == 0, mean, jnp.where(lane == 1, spread, 0.0))
+    both = jnp.concatenate([both, jnp.zeros((PAD_TOK - TOK, LANES), f32)], axis=0).T[:8, :]
+    gain_row = jnp.concatenate([norm_gain[...], norm_gain[...]], axis=1)
+    message[...] = jnp.where(iota((8, PAD_TOK), 0) == 2, gain_row, both)
+    me = y * SIDE + x
+    for mate in mates:
+        copy_to(message, stats.at[me], stat_send, stat_recv, mate).start()
+    stats[me] = message[...]
+    fetches[3].wait()
+    most = stats.at[pl.ds(0, SIDE * SIDE - 1)]
+    arrived = copy_to(most, most, stat_send, stat_recv, mates[0])
+    arrived.wait_recv()
+    means = stats[:, 0, :]
+    gains[...] = stats[:, 2, :LANES]
+    mean = jnp.mean(means, axis=0, keepdims=True)
+    apart = means - mean
+    var = (
+        jnp.sum(stats[:, 1, :], axis=0, keepdims=True) + LANES * jnp.sum(apart * apart, axis=0, keepdims=True)
+    ) / WIDE
+    inverse = lax.rsqrt(var + epsilon)
+    mean_t = jnp.broadcast_to(mean, (LANES, PAD_TOK)).T[:TOK, :]
+    inverse_t = jnp.broadcast_to(inverse, (LANES, PAD_TOK)).T[:TOK, :]
+    act = jax.nn.silu((conv[...] - mean_t) * inverse_t * chan_gain[...]).astype(bf16)
+
+    for j in range(SIDE * SIDE // 2):
+        pair = jnp.dot(
+            act, pointw[:, 2 * j * LANES : 2 * (j + 1) * LANES], preferred_element_type=f32
+        ).astype(bf16)
+        for k in range(2):
+            b = 2 * j + k
+            mix_part[b // SIDE, b % SIDE, :, :] = pair[:, k * LANES : (k + 1) * LANES]
+    mlands = (mland0, mland1, mland2, mland3)
+    count = TOK // MIX_CHUNKS
+    mreduces = [Reduce(plane, mix_part, c * count, count, mlands, mrs_send, mrs_recv, c) for c in range(MIX_CHUNKS)]
+    mgathers = [Gather(plane, mix_rows, c * count, count, mag_send, mag_recv, c) for c in range(MIX_CHUNKS)]
+    for step in range(4):
+        for c in range(MIX_CHUNKS):
+            mreduces[c].issue(step)
+    for c in range(MIX_CHUNKS):
+        for color in range(2):
+            mix_rows[y, x, mreduces[c].rows(color), :] = mreduces[c].total(color).astype(bf16)
+        mgathers[c].issue(0)
+    for c in range(MIX_CHUNKS):
+        mgathers[c].issue(1)
+    for c in range(MIX_CHUNKS):
+        mgathers[c].arrived(1)
+        mgathers[c].issue(2)
+    for c in range(MIX_CHUNKS):
+        mgathers[c].issue(3)
+    for c in range(MIX_CHUNKS):
+        mgathers[c].arrived(3)
+
+    squares = jnp.zeros((TOK, LANES), f32)
+    for b in range(SIDE * SIDE):
+        block = mix_rows[b // SIDE, b % SIDE].astype(f32)
+        squares = squares + block * block
+    scale = lax.rsqrt(jnp.sum(squares, axis=1, keepdims=True) / WIDE + epsilon)
+    left = jnp.concatenate([mix_rows[b // SIDE, b % SIDE] for b in range(SIDE * SIDE)], axis=1)
+    branch = jnp.dot(left, scaled_out[...], preferred_element_type=f32) * scale
+    fetches[5].wait()
+    mid[...] = (resid[...].astype(f32) + branch).astype(bf16)
+    picked = jnp.dot(picker[...], mid[...], preferred_element_type=f32).astype(bf16)
+    outgoing[...] = picked.reshape(E, CAP, LANES)
 
     other = 1 - core
     for i, offset in enumerate(OFFSETS):
         chip = lax.rem(z - offset + CHIPS, CHIPS)
-        place = pl.ds(pl.multiple_of((2 * i + core) * CAP, CAP), CAP)
+        spot = pl.ds(pl.multiple_of((2 * i + core) * CAP, CAP), CAP)
         for way in range(2):
             if i == 0 and way == 1:
                 continue
             target = 2 * chip + (other if i == 0 else way)
             copy_to(
                 outgoing.at[target],
-                rows.at[y, x, place, :],
+                rows.at[y, x, spot, :],
                 out_send,
                 out_recv.at[2 * i // PERCHUNK],
                 {"sp": target},
@@ -269,46 +462,44 @@
     def begin(c):
         count = CROWS - (CAP if c == 0 else 0)
         landed = rows.at[y, x, pl.ds(c * CROWS, count), :]
-        copy_to(landed, landed, out_send, out_recv.at[c], {"sp": sp}).wait_recv()
+        copy_to(landed, landed, out_send, out_recv.at[c], {"sp": lax.rem(sp + 1, E)}).wait_recv()
         gathers[c].issue(0)
 
     def compute(c):
         gathers[c].arrived(3)
         if c == 0:
-            for fetch in fetches:
+            for fetch in fetches[6:]:
                 fetch.wait()
         step = 32
 
         @pl.loop(0, CROWS // step)
         def _(i):
             at = pl.multiple_of(i * step, step)
-            block = rows[:, :, pl.ds(c * CROWS + at, step), :].astype(jnp.float32)
+            block = rows[:, :, pl.ds(c * CROWS + at, step), :].astype(f32)
             block = block.reshape(SIDE * SIDE, step, LANES)
             squares = jnp.sum(jnp.sum(block * block, axis=0), axis=1, keepdims=True)
-            scale = lax.rsqrt(squares / (SIDE * SIDE * LANES) + epsilon)
-            scaled = block * scale[None] * gain[...][:, None, :]
-            normed[:, pl.ds(at, step), :] = scaled.astype(jnp.bfloat16)
+            scale = lax.rsqrt(squares / WIDE + epsilon)
+            scaled = block * scale[None] * gains[...][:, None, :]
+            normed[:, pl.ds(at, step), :] = scaled.astype(bf16)
 
         left = jnp.concatenate([normed[b] for b in range(SIDE * SIDE)], axis=1)
-        gate_pre = jnp.minimum(jnp.dot(left, gate[...], preferred_element_type=jnp.float32), clamp_limit)
-        up_pre = jnp.clip(
-            jnp.dot(left, up[...], preferred_element_type=jnp.float32), -clamp_limit, clamp_limit
-        )
-        hidden = (gate_pre * jax.nn.sigmoid(swish_slope * gate_pre) * (up_pre + 1.0)).astype(jnp.bfloat16)
-        place = pl.ds(c * CROWS, CROWS)
+        gate_pre = jnp.minimum(jnp.dot(left, gate[...], preferred_element_type=f32), clamp_limit)
+        up_pre = jnp.clip(jnp.dot(left, up[...], preferred_element_type=f32), -clamp_limit, clamp_limit)
+        hidden = (gate_pre * jax.nn.sigmoid(swish_slope * gate_pre) * (up_pre + 1.0)).astype(bf16)
+        spot = pl.ds(c * CROWS, CROWS)
         for j in range(SIDE * SIDE // 2):
-            both = jnp.dot(
-                hidden, down[:, 2 * j * LANES : 2 * (j + 1) * LANES], preferred_element_type=jnp.float32
-            ).astype(jnp.bfloat16)
+            pair = jnp.dot(
+                hidden, down[:, 2 * j * LANES : 2 * (j + 1) * LANES], preferred_element_type=f32
+            ).astype(bf16)
             for k in range(2):
                 b = 2 * j + k
-                partial[b // SIDE, b % SIDE, place, :] = both[:, k * LANES : (k + 1) * LANES]
+                partial[b // SIDE, b % SIDE, spot, :] = pair[:, k * LANES : (k + 1) * LANES]
         reduces[c].issue(0)
 
     def finish(c):
         half = CROWS // 2
         for color in range(2):
-            total[pl.ds(c * CROWS + color * half, half), :] = reduces[c].total(color).astype(jnp.bfloat16)
+            total[pl.ds(c * CROWS + color * half, half), :] = reduces[c].total(color).astype(bf16)
         for p in range(c * PERCHUNK, (c + 1) * PERCHUNK):
             i, way = p // 2, p % 2
             if i == 0 and way == 1:
@@ -342,98 +533,19 @@
                 stages[stage](c)
 
     whole = back.at[pl.ds(0, E - 1)]
-    copy_to(whole, whole, back_send, back_recv, {"sp": sp}).wait_recv()
+    copy_to(whole, whole, back_send, back_recv, {"sp": lax.rem(sp + 1, E)}).wait_recv()
     values = back[...].reshape(ROWS, LANES)
-    routed = jnp.dot(mix_hi[...], values, preferred_element_type=jnp.float32)
-    routed = routed + jnp.dot(mix_lo[...], values, preferred_element_type=jnp.float32)
-    result[...] = (middle[...].astype(jnp.float32) + routed).astype(jnp.bfloat16)
-
+    routed = jnp.dot(mixer_hi[...], values, preferred_element_type=f32)
+    routed = routed + jnp.dot(mixer_lo[...], values, preferred_element_type=f32)
+    result[...] = (mid[...].astype(f32) + routed).astype(bf16)
+
+    arrived.wait_send()
     sent = outgoing.at[pl.ds(0, E - 1)]
-    copy_to(sent, sent, out_send, out_recv.at[0], {"sp": sp}).wait_send()
+    copy_to(sent, sent, out_send, out_recv.at[0], {"sp": lax.rem(sp + 1, E)}).wait_send()
     sent = total.at[pl.ds(0, ROWS - CAP), :]
-    copy_to(sent, sent, back_send, back_recv, {"sp": sp}).wait_send()
-    for c in range(CHUNKS):
-        gathers[c].sent()
-        reduces[c].sent()
-
-
-def experts(outgoing, middle, mix_hi, mix_lo, gain, gate_experts, up_experts, down_experts):
-    vmem = pl.BlockSpec(memory_space=pltpu.VMEM)
-    hbm = pl.BlockSpec(memory_space=pl.ANY)
-    bf16 = jnp.bfloat16
-    depth, hidden = gate_experts.shape[1], gate_experts.shape[2]
-    sems = pltpu.SemaphoreType.DMA((CHUNKS, 2, 4, 2))
-    one = pltpu.SemaphoreType.DMA
-    return pl.pallas_call(
-        expert_kernel,
-        out_shape=jax.ShapeDtypeStruct(middle.shape, bf16),
-        in_specs=[vmem] * 5 + [hbm] * 3,
-        out_specs=vmem,
-        scratch_shapes=[
-            pltpu.VMEM((depth, hidden), bf16),
-            pltpu.VMEM((depth, hidden), bf16),
-            pltpu.VMEM((hidden, depth), bf16),
-            pltpu.VMEM((SIDE, SIDE, ROWS, LANES), bf16),
-            pltpu.VMEM((SIDE * SIDE, CROWS, LANES), bf16),
-            pltpu.VMEM((SIDE, SIDE, ROWS, LANES), bf16),
-            *land_shapes(CHUNKS, CROWS),
-            pltpu.VMEM((ROWS, LANES), bf16),
-            pltpu.VMEM((E, CAP, LANES), bf16),
-            one((3,)),
-            sems,
-            sems,
-            sems,
-            sems,
-            one,
-            one((CHUNKS,)),
-            one,
-            one,
-        ],
-        compiler_params=pltpu.CompilerParams(
-            collective_id=1, has_side_effects=True, vmem_limit_bytes=48 * 1024 * 1024
-        ),
-        name="experts",
-    )(outgoing, middle, mix_hi, mix_lo, gain, gate_experts, up_experts, down_experts)
-
-
-def from_behind(block, axis, distance):
-    devices = range(lax.axis_size(axis))
-    route = [(i - distance, i) for i in devices if i - distance in devices]
-    return lax.ppermute(block, axis, route)
-
-
-def over_axes(value, axes):
-    for axis in axes:
-        value = lax.psum(value, axis)
-    return value
-
-
-def split_up(value, dim, count):
-    dims = value.shape
-    pieces = value.reshape(*dims[:dim], count, dims[dim] // count, *dims[dim + 1 :])
-    return jnp.moveaxis(pieces, dim, 0)
-
-
-def summed_on_arrival(value, axis, dim):
-    pieces = split_up(value, dim, lax.axis_size(axis))
-    arrived = lax.all_to_all(pieces, axis, split_axis=0, concat_axis=0, tiled=True)
-    return arrived.astype(jnp.float32).sum(axis=0)
-
-
-def from_everyone(value, axis):
-    copies = jnp.broadcast_to(value, (lax.axis_size(axis), *value.shape))
-    return lax.all_to_all(copies, axis, split_axis=0, concat_axis=0, tiled=True)
-
-
-def laid_out(pieces, dim):
-    dims = list(pieces.shape[1:])
-    dims[dim] *= pieces.shape[0]
-    return jnp.moveaxis(pieces, 0, dim).reshape(dims)
-
-
-def gathered_copies(value, axis, dim):
-    pieces = from_everyone(value, axis)
-    return laid_out(pieces, dim)
+    copy_to(sent, sent, back_send, back_recv, {"sp": lax.rem(sp + 1, E)}).wait_send()
+    for op in (*mreduces, *mgathers, *gathers, *reduces):
+        op.sent()
 
 
 def shards(
@@ -452,55 +564,82 @@
     up_experts,
     down_experts,
 ):
-    tok_rows, chan_local = conv_value.shape
-    feat_local = resid.shape[1]
-    lookback = depth_kernel.shape[0] - 1
-    gated = (conv_value.astype(jnp.float32) * jax.nn.sigmoid(conv_gate.astype(jnp.float32))).astype(
-        jnp.bfloat16
-    )
-    earlier = from_behind(gated[tok_rows - lookback :], "sp", 1)
-    padded = jnp.concatenate([earlier, gated], axis=0)
-    conv = jnp.zeros((tok_rows, chan_local), jnp.float32)
-    for tap in range(lookback + 1):
-        conv = conv + padded[tap : tap + tok_rows].astype(jnp.float32) * depth_kernel[tap]
-    chan_total = chan_local * lax.axis_size(TP)
-    row_sums, row_squares = (
-        over_axes(jnp.sum(conv, axis=1), TP),
-        over_axes(jnp.sum(conv * conv, axis=1), TP),
-    )
-    row_mean = row_sums / chan_total
-    row_var = row_squares / chan_total - row_mean * row_mean
-    act = jax.nn.silu(
-        (conv - row_mean[:, None]) * lax.rsqrt(row_var[:, None] + epsilon) * chan_gain
-    ).astype(jnp.bfloat16)
-    point = summed_on_arrival(
-        jnp.dot(act, point_weight, preferred_element_type=jnp.float32).astype(jnp.bfloat16), TP, 0
-    )
-    mixed = (
-        point * lax.rsqrt(jnp.mean(point * point, axis=1, keepdims=True) + epsilon) * mix_gain
-    ).astype(jnp.bfloat16)
-    branch = jnp.dot(gathered_copies(mixed, TP, 0), out_weight, preferred_element_type=jnp.float32)
-    middle = (resid.astype(jnp.float32) + branch).astype(jnp.bfloat16)
-    gain = from_everyone(norm_gain, TP).reshape(SIDE * SIDE, LANES)
-
-    flat_ids = route_ids.reshape(-1)
-    expert_table = (flat_ids[:, None] == jnp.arange(E, dtype=jnp.int32)[None, :]).astype(jnp.int32)
-    earlier_count = jnp.cumsum(expert_table, axis=0) - expert_table
-    position = jnp.sum(earlier_count * expert_table, axis=1)
-    slot_grid = (flat_ids * CAP + position).reshape(tok_rows, TOPK)
-    hits = slot_grid[None, :, :] == jnp.arange(E * CAP, dtype=jnp.int32)[:, None, None]
-    picker = jnp.any(hits, axis=2).astype(jnp.bfloat16)
-    outgoing = (
-        jnp.dot(picker, middle, preferred_element_type=jnp.float32)
-        .astype(jnp.bfloat16)
-        .reshape(E, CAP, feat_local)
-    )
-    back_hits = slot_grid[:, :, None] == jnp.arange(E * CAP, dtype=jnp.int32)[None, None, :]
-    mixer = jnp.sum(jnp.where(back_hits, route_weights[:, :, None], 0.0), axis=1)
-    mix_hi = lax.reduce_precision(mixer, 8, 7)
-    mix_lo = (mixer - mix_hi).astype(jnp.bfloat16)
-    return experts(
-        outgoing, middle, mix_hi.astype(jnp.bfloat16), mix_lo, gain, gate_experts, up_experts, down_experts
+    routes = jnp.concatenate([route_ids.T.astype(jnp.float32), route_weights.T], axis=0)
+    routes = jnp.pad(routes, ((0, 0), (0, PAD_TOK - TOK)))
+    vmem = pl.BlockSpec(memory_space=pltpu.VMEM)
+    hbm = pl.BlockSpec(memory_space=pl.ANY)
+    f32, bf16 = jnp.float32, jnp.bfloat16
+    depth, hidden = gate_experts.shape[1], gate_experts.shape[2]
+    sems = pltpu.SemaphoreType.DMA((CHUNKS, 2, 4, 2))
+    msems = pltpu.SemaphoreType.DMA((MIX_CHUNKS, 2, 4, 2))
+    one = pltpu.SemaphoreType.DMA
+    fed = (conv_value, conv_gate, depth_kernel, resid, point_weight, out_weight)
+    experts = (gate_experts, up_experts, down_experts)
+    return pl.pallas_call(
+        layer_kernel,
+        out_shape=jax.ShapeDtypeStruct(resid.shape, bf16),
+        in_specs=[hbm] * 9 + [vmem] * 4,
+        out_specs=vmem,
+        scratch_shapes=[
+            *(pltpu.VMEM(a.shape, a.dtype) for a in fed),
+            *(pltpu.VMEM(a.shape[1:], a.dtype) for a in experts),
+            pltpu.VMEM((HALO + TOK, LANES), f32),
+            pltpu.VMEM((HALO, LANES), f32),
+            pltpu.VMEM((TOK, LANES), f32),
+            pltpu.VMEM((8, PAD_TOK), f32),
+            pltpu.VMEM((SIDE * SIDE, 8, PAD_TOK), f32),
+            pltpu.VMEM((SIDE * SIDE, LANES), f32),
+            pltpu.VMEM((depth, LANES), bf16),
+            pltpu.VMEM((ROWS, TOK), bf16),
+            pltpu.VMEM((TOK, ROWS), bf16),
+            pltpu.VMEM((TOK, ROWS), bf16),
+            pltpu.VMEM((TOK, LANES), bf16),
+            pltpu.VMEM((E, CAP, LANES), bf16),
+            pltpu.VMEM((SIDE, SIDE, TOK, LANES), bf16),
+            pltpu.VMEM((SIDE, SIDE, TOK, LANES), bf16),
+            *land_shapes(MIX_CHUNKS, TOK // MIX_CHUNKS),
+            pltpu.VMEM((SIDE, SIDE, ROWS, LANES), bf16),
+            pltpu.VMEM((SIDE * SIDE, CROWS, LANES), bf16),
+            pltpu.VMEM((SIDE, SIDE, ROWS, LANES), bf16),
+            *land_shapes(CHUNKS, CROWS),
+            pltpu.VMEM((ROWS, LANES), bf16),
+            pltpu.VMEM((E, CAP, LANES), bf16),
+            one((9,)),
+            one,
+            one,
+            one,
+            one,
+            msems,
+            msems,
+            msems,
+            msems,
+            sems,
+            sems,
+            sems,
+            sems,
+            one,
+            one((CHUNKS,)),
+            one,
+            one,
+        ],
+        compiler_params=pltpu.CompilerParams(
+            collective_id=1, has_side_effects=True, vmem_limit_bytes=48 * 1024 * 1024
+        ),
+        name="layer",
+    )(
+        conv_value,
+        conv_gate,
+        depth_kernel,
+        resid,
+        point_weight,
+        out_weight,
+        gate_experts,
+        up_experts,
+        down_experts,
+        chan_gain.reshape(1, LANES),
+        mix_gain.reshape(SIDE * SIDE, LANES),
+        norm_gain.reshape(1, LANES),
+        routes,
     )
 
 

time: 177 us -> 142 us (0.80)
  Pallas kernels: 97.7 us -> 132 us
  waiting for transfers between devices: 28.2 us -> 0 us
  starting transfers between devices: 16.4 us -> 0 us
  blocking collectives: 15.3 us -> 0 us
  other arithmetic: 5.45 us -> 0.74 us
  matrix products: 4.04 us -> 0 us
    pallas_call x1, Pallas kernels: 97.7 us -> 132 us  [shards(): pl.pallas_call(layer_kernel, out_shape=jax.ShapeDtypeStruct(resid.shape,...]
    all_to_all x3 -> x0, waiting for transfers between devices: 26.3 us -> none  [the longest x2 14.3 us: from_everyone(): return lax.all_to_all(copies, axis, split_axis=0, concat_axis=0, tiled=True)]
    psum x2 -> x0, blocking collectives: 15.3 us -> none  [over_axes(): value = lax.psum(value, axis)]
    all_to_all x3 -> x0, starting transfers between devices: 11.5 us -> none  [the longest x2 7.68 us: from_everyone(): return lax.all_to_all(copies, axis, split_axis=0, concat_axis=0, tiled=True)]
    unnamed x24 -> x27, local copies, waits for them, and re-layouts: 2.96 us -> 9.47 us
    ppermute x1 -> x0, starting transfers between devices: 4.92 us -> none  [from_behind(): return lax.ppermute(block, axis, route)]
    dot_general x3 -> x0, matrix products: 4.04 us -> none  [the longest x1 1.73 us: shards(): jnp.dot(gathered_copies(mixed, TP, 0), out_weight, preferred_element_type...]
    reshape x2 -> x0, local copies, waits for them, and re-layouts: 2.21 us -> none  [the longest x1 1.16 us: split_up(): value.reshape(*dims[:dim], count, dims[dim] // count, *dims[dim + 1:])]
  transfers between devices with their start and end apart: 4 -> 0, of which waited for: 4 -> 0; matrix products, arithmetic and copies ran while one was open for 6% -> 0% of each run, Pallas kernels for 0% -> 0%
where the time goes in v2:
time: 142 us
  Pallas kernels  132 us (93%)
  local copies, waits for them, and re-layouts  9.47 us (7%)
    pallas_call x1, Pallas kernels, shards(): pl.pallas_call(layer_kernel, out_shape=jax.ShapeDtypeStruct(resid.shape,...  132 us
    unnamed x27, local copies, waits for them, and re-layouts  9.47 us

profile of v2, /device:TPU:1, one launch (start us, length us, event | category | flops | bytes accessed | tf_op | source)
XLA Modules:
  0.0 141.9 jit_solution(9332842859918311922)
XLA Ops:
  0.0 0.0 copy-start.12
  0.0 0.0 copy-start.8
  0.0 0.7 copy-done.12
  0.7 0.0 copy-start.9
  0.7 0.0 copy-start.10
  0.7 0.0 copy-start.11
  0.7 0.7 select_maximum_fusion.routes
  1.4 0.0 copy-done.8
  1.4 0.0 copy-done.9
  1.4 0.0 copy-done.10
  1.5 0.0 copy-done.11
  1.5 0.0 copy-start
  1.5 1.2 copy-done
  2.7 0.0 copy-start.1
  2.7 1.2 copy-done.1
  3.9 0.0 copy-start.2
  3.9 1.2 copy-done.2
  5.1 0.0 copy-start.3
  5.1 1.0 copy-done.3
  6.2 0.0 copy-start.4
  6.2 1.0 copy-done.4
  7.2 0.0 copy-start.5
  7.2 0.8 copy-done.5
  8.0 0.0 copy-start.6
  8.0 0.8 copy-done.6
  8.8 0.0 copy-start.7
  8.8 0.8 copy-done.7
  9.6 131.6 %layer.1 = bf16[192,128]{1,0:T(8,128)(2,1)S(1)} custom-call(bf16[192,128]{1,0:T(8,128)(2,1)S(1)} %copy-done.5, bf16[192,128]{1,0:T(8,128)(2,1)S(1)} %copy-done.6, f32[31,128]{1,0:T(8,128)S(1)} %copy-done.8, bf16[192,128]{1,0:T(8,128)(2,1)S(1)} %copy-done.7, bf16[128,2048]{1,0:T(8,128)(2,1)S(1)} %copy-done.3, bf16[2048,128]{1,0:T(8,128)(2,1)S(1)} %copy-done.4, ...), custom_call_target="tpu_custom_call" | custom-call | tf_op jit(solution)/shard_map/layer/pallas_call | solution.py:578
  141.3 0.6 copy.16
  (1 shorter events, 0.0 us)
Async XLA Ops:
  0.0 0.7 copy-start.12
  0.0 1.4 %copy-start.8 = (f32[31,128]{1,0:T(8,128)S(1)}, f32[31,128]{1,0:T(8,128)}, u32[]{:S(2)}) copy-start(f32[31,128]{1,0:T(8,128)} %taps_hbm.1) | copy-start | bytes 47620
  0.7 0.7 copy-start.9
  0.7 0.8 copy-start.10
  0.7 0.8 copy-start.11
  1.5 1.2 copy-start
  2.7 1.2 copy-start.1
  3.9 1.2 copy-start.2
  5.1 1.0 copy-start.3
  6.2 1.0 copy-start.4
  7.2 0.8 copy-start.5
  8.0 0.8 copy-start.6
  8.8 0.8 copy-start.7

commit v3 on v2

--- a/solution.py
+++ b/solution.py
@@ -253,6 +253,7 @@
     total,
     back,
     fetch_sem,
+    round_sem,
     halo_send,
     halo_recv,
     stat_send,
@@ -278,16 +279,13 @@
 
     barrier = pltpu.get_barrier_semaphore()
 
-    @pl.loop(1, E)
-    def _(d):
-        pl.semaphore_signal(barrier, inc=1, device_id={"sp": lax.rem(sp + d, E)}, device_id_type=MESH)
-
     mates = []
     for dy in range(SIDE):
         for dx in range(SIDE):
             if dy or dx:
                 mates.append({"tp_0": lax.rem(y + dy, SIDE), "tp_1": lax.rem(x + dx, SIDE)})
-    for mate in mates:
+    close = [{"sp": lax.rem(sp + d + E, E)} for d in (1, -1, 2, -2)]
+    for mate in mates + close:
         pl.semaphore_signal(barrier, inc=1, device_id=mate, device_id_type=MESH)
 
     fetches = []
@@ -308,6 +306,49 @@
         fetch.start()
         fetches.append(fetch)
 
+    def mixer_table():
+        packed = routes[...]
+        turned = jnp.concatenate([packed, jnp.zeros((LANES - 8, PAD_TOK), f32)], axis=0).T
+        lanes_e = iota((TOK, E), 1).astype(f32)
+        member = jnp.zeros((TOK, E), f32)
+        weight = jnp.zeros((TOK, E), f32)
+        for k in range(TOPK):
+            hit = turned[:TOK, k : k + 1] == lanes_e
+            member = jnp.where(hit, 1.0, member)
+            weight = jnp.where(hit, turned[:TOK, TOPK + k : TOPK + k + 1], weight)
+        before = (iota((TOK, TOK), 1) < iota((TOK, TOK), 0)).astype(f32).astype(bf16)
+        place = jnp.dot(before, member.astype(bf16), preferred_element_type=f32)
+        place = jnp.where(member > 0.0, place, -1.0).astype(bf16)
+        weight_hi = weight.astype(bf16)
+        weight_lo = (weight - weight_hi.astype(f32)).astype(bf16)
+        for g in range(ROWS // LANES):
+            spread_to = (iota((E, LANES), 1) // CAP + g * (LANES // CAP) == iota((E, LANES), 0)).astype(f32).astype(bf16)
+            slots = jnp.dot(place, spread_to, preferred_element_type=f32)
+            mine = slots == lax.rem(iota((TOK, LANES), 1), CAP).astype(f32)
+            for part, held in ((weight_hi, mixer_hi), (weight_lo, mixer_lo)):
+                wide = jnp.dot(part, spread_to, preferred_element_type=f32)
+                held[:, g * LANES : (g + 1) * LANES] = jnp.where(mine, wide, 0.0).astype(bf16)
+
+    def picker_table():
+        packed = routes[...]
+        tall_e = iota((E, TOK), 0).astype(f32)
+        member = jnp.zeros((E, TOK), f32)
+        for k in range(TOPK):
+            member = jnp.where(packed[k : k + 1, :TOK] == tall_e, 1.0, member)
+        after = (iota((TOK, TOK), 0) < iota((TOK, TOK), 1)).astype(f32).astype(bf16)
+        place = jnp.dot(member.astype(bf16), after, preferred_element_type=f32)
+        place = jnp.where(member > 0.0, place, -1.0)
+        tall_c = iota((CAP, TOK), 0).astype(f32)
+        for e in range(E):
+            picker[e * CAP : (e + 1) * CAP, :] = (place[e : e + 1, :] == tall_c).astype(f32).astype(bf16)
+
+    def scale_out():
+        fetches[4].wait()
+        columns = jnp.concatenate([mix_gain[...], jnp.zeros((LANES - SIDE * SIDE, LANES), f32)], axis=0).T
+        for b in range(SIDE * SIDE):
+            part = slice(b * LANES, (b + 1) * LANES)
+            scaled_out[part, :] = (outw[part, :].astype(f32) * columns[:, b : b + 1]).astype(bf16)
+
     for i in range(3):
         fetches[i].wait()
     unit = value[...].astype(f32) * jax.nn.sigmoid(gating[...].astype(f32))
@@ -322,50 +363,24 @@
 
     conv[HALO:, :] = convolve(HALO, TOK - HALO)
 
-    packed = routes[...]
-    turned = jnp.concatenate([packed, jnp.zeros((LANES - 8, PAD_TOK), f32)], axis=0).T
-    lanes_e = iota((TOK, E), 1).astype(f32)
-    member = jnp.zeros((TOK, E), f32)
-    weight = jnp.zeros((TOK, E), f32)
-    for k in range(TOPK):
-        hit = turned[:TOK, k : k + 1] == lanes_e
-        member = jnp.where(hit, 1.0, member)
-        weight = jnp.where(hit, turned[:TOK, TOPK + k : TOPK + k + 1], weight)
-    before = (iota((TOK, TOK), 1) < iota((TOK, TOK), 0)).astype(f32).astype(bf16)
-    place = jnp.dot(before, member.astype(bf16), preferred_element_type=f32)
-    place = jnp.where(member > 0.0, place, -1.0).astype(bf16)
-    weight_hi = weight.astype(bf16)
-    weight_lo = (weight - weight_hi.astype(f32)).astype(bf16)
-    for g in range(ROWS // LANES):
-        spread_to = (iota((E, LANES), 1) // CAP + g * (LANES // CAP) == iota((E, LANES), 0)).astype(f32).astype(bf16)
-        slots = jnp.dot(place, spread_to, preferred_element_type=f32)
-        mine = slots == lax.rem(iota((TOK, LANES), 1), CAP).astype(f32)
-        for part, held in ((weight_hi, mixer_hi), (weight_lo, mixer_lo)):
-            wide = jnp.dot(part, spread_to, preferred_element_type=f32)
-            held[:, g * LANES : (g + 1) * LANES] = jnp.where(mine, wide, 0.0).astype(bf16)
-
-    tall_e = iota((E, TOK), 0).astype(f32)
-    member = jnp.zeros((E, TOK), f32)
-    for k in range(TOPK):
-        member = jnp.where(packed[k : k + 1, :TOK] == tall_e, 1.0, member)
-    after = (iota((TOK, TOK), 0) < iota((TOK, TOK), 1)).astype(f32).astype(bf16)
-    place = jnp.dot(member.astype(bf16), after, preferred_element_type=f32)
-    place = jnp.where(member > 0.0, place, -1.0)
-    tall_c = iota((CAP, TOK), 0).astype(f32)
-    for e in range(E):
-        picker[e * CAP : (e + 1) * CAP, :] = (place[e : e + 1, :] == tall_c).astype(f32).astype(bf16)
-
-    fetches[4].wait()
-    columns = jnp.concatenate([mix_gain[...], jnp.zeros((LANES - SIDE * SIDE, LANES), f32)], axis=0).T
-    for b in range(SIDE * SIDE):
-        part = slice(b * LANES, (b + 1) * LANES)
-        scaled_out[part, :] = (outw[part, :].astype(f32) * columns[:, b : b + 1]).astype(bf16)
-
-    pl.semaphore_wait(barrier, E - 1 + len(mates))
+    pl.semaphore_wait(barrier, len(mates) + len(close))
+
+    def hear(r):
+        pl.semaphore_wait(round_sem.at[r], 2)
+
+    def tell(r):
+        for d in (2 ** (r + 1), -(2 ** (r + 1))):
+            pl.semaphore_signal(
+                round_sem.at[r], inc=1, device_id={"sp": lax.rem(sp + d + E, E)}, device_id_type=MESH
+            )
+
+    tell(0)
 
     tail = copy_to(padded.at[pl.ds(TOK, HALO), :], halo, halo_send, halo_recv, {"sp": lax.rem(sp + 1, E)})
     tail.start()
     tail.wait()
+    hear(0)
+    tell(1)
     padded[:HALO, :] = jnp.where(sp > 0, halo[...], 0.0)
     conv[:HALO, :] = convolve(0, HALO)
 
@@ -381,6 +396,9 @@
     for mate in mates:
         copy_to(message, stats.at[me], stat_send, stat_recv, mate).start()
     stats[me] = message[...]
+    mixer_table()
+    hear(1)
+    tell(2)
     fetches[3].wait()
     most = stats.at[pl.ds(0, SIDE * SIDE - 1)]
     arrived = copy_to(most, most, stat_send, stat_recv, mates[0])
@@ -411,6 +429,10 @@
     for step in range(4):
         for c in range(MIX_CHUNKS):
             mreduces[c].issue(step)
+        if step == 0:
+            picker_table()
+        if step == 1:
+            scale_out()
     for c in range(MIX_CHUNKS):
         for color in range(2):
             mix_rows[y, x, mreduces[c].rows(color), :] = mreduces[c].total(color).astype(bf16)
@@ -437,6 +459,7 @@
     picked = jnp.dot(picker[...], mid[...], preferred_element_type=f32).astype(bf16)
     outgoing[...] = picked.reshape(E, CAP, LANES)
 
+    hear(2)
     other = 1 - core
     for i, offset in enumerate(OFFSETS):
         chip = lax.rem(z - offset + CHIPS, CHIPS)
@@ -567,7 +590,7 @@
     routes = jnp.concatenate([route_ids.T.astype(jnp.float32), route_weights.T], axis=0)
     routes = jnp.pad(routes, ((0, 0), (0, PAD_TOK - TOK)))
     vmem = pl.BlockSpec(memory_space=pltpu.VMEM)
-    hbm = pl.BlockSpec(memory_space=pl.ANY)
+    hbm = pl.BlockSpec(memory_space=pltpu.HBM)
     f32, bf16 = jnp.float32, jnp.bfloat16
     depth, hidden = gate_experts.shape[1], gate_experts.shape[2]
     sems = pltpu.SemaphoreType.DMA((CHUNKS, 2, 4, 2))
@@ -605,6 +628,7 @@
             pltpu.VMEM((ROWS, LANES), bf16),
             pltpu.VMEM((E, CAP, LANES), bf16),
             one((9,)),
+            pltpu.SemaphoreType.REGULAR((3,)),
             one,
             one,
             one,
@@ -623,7 +647,7 @@
             one,
         ],
         compiler_params=pltpu.CompilerParams(
-            collective_id=1, has_side_effects=True, vmem_limit_bytes=48 * 1024 * 1024
+            collective_id=1, has_side_effects=True, vmem_limit_bytes=67043328
         ),
         name="layer",
     )(

time: 142 us -> 134 us (0.944)
  local copies, waits for them, and re-layouts: 9.47 us -> 2.79 us
  Pallas kernels: 132 us -> 130 us
    unnamed x27 -> x5, local copies, waits for them, and re-layouts: 9.47 us -> 2.79 us
where the time goes in v3:
time: 134 us
  Pallas kernels  130 us (97%)
  local copies, waits for them, and re-layouts  2.79 us (2%)
    pallas_call x1, Pallas kernels, shards(): pl.pallas_call(layer_kernel, out_shape=jax.ShapeDtypeStruct(resid.shape,...  130 us
    unnamed x5, local copies, waits for them, and re-layouts  2.79 us

profile of v3, /device:TPU:1, one launch (start us, length us, event | category | flops | bytes accessed | tf_op | source)
XLA Modules:
  0.0 133.8 jit_solution(9796306005748577389)
XLA Ops:
  0.0 0.0 copy-start
  0.0 0.7 copy-done
  0.7 0.0 copy-start.1
  0.7 0.7 copy-done.1
  1.4 0.6 select_maximum_fusion.routes
  2.0 130.4 %layer.1 = bf16[192,128]{1,0:T(8,128)(2,1)} custom-call(bf16[192,128]{1,0:T(8,128)(2,1)} %value_hbm.1, bf16[192,128]{1,0:T(8,128)(2,1)} %gating_hbm.1, f32[31,128]{1,0:T(8,128)} %taps_hbm.1, bf16[192,128]{1,0:T(8,128)(2,1)} %resid_hbm.1, bf16[128,2048]{1,0:T(8,128)(2,1)} %point_hbm.1, bf16[2048,128]{1,0:T(8,128)(2,1)} %outw_hbm.1, ...), custom_call_target="tpu_custom_call" | custom-call | tf_op jit(solution)/shard_map/layer/pallas_call | solution.py:601
  132.4 1.4 %copy.16 = bf16[192,128]{1,0:T(8,128)(2,1)} copy(bf16[192,128]{1,0:T(8,128)(2,1)} %layer.1) | data formatting | bytes 98304
  (1 shorter events, 0.0 us)
Async XLA Ops:
  0.0 0.7 copy-start
  0.7 0.7 copy-start.1

commit v4 on v3

--- a/solution.py
+++ b/solution.py
@@ -23,7 +23,7 @@
 CHUNKS = 4
 CROWS = ROWS // CHUNKS
 PERCHUNK = CROWS // CAP
-OFFSETS = [0, 1, -1, 2, -2, 3, -3, 4, -4, 5, -5, 6, -6, 7, -7, 8]
+OFFSETS = [0, 1, -1, 2, -4, 5, -5, 6, -6, 7, -7, 8, -2, 3, -3, 4]
 
 
 class Plane:
@@ -55,8 +55,8 @@
 
 
 class Gather:
-    def __init__(self, plane, buf, base, count, send, recv, chunk):
-        self.plane, self.buf, self.chunk = plane, buf, chunk
+    def __init__(self, plane, buf, base, count, send, recv, chunk, direct=False):
+        self.plane, self.buf, self.chunk, self.direct = plane, buf, chunk, direct
         self.send, self.recv = send, recv
         self.half = count // 2
         self.quarter = count // 4
@@ -89,6 +89,11 @@
                 block = view(self.buf, dim, plane.pos[dim], self.rows(color))
                 self.go(color, step, 0, block, block, ahead)
                 self.go(color, step, 1, block, block, behind)
+                if self.direct and step == 0:
+                    self.go(color, 1, 0, block, block, plane.neighbour(dim, 2))
+            elif self.direct and step == 1:
+                for way in range(2):
+                    self.pending[(color, 0, way)].wait_recv()
             else:
                 self.pending[(color, step - 1, 0)].wait_recv()
                 block = view(self.buf, dim, plane.at(dim, -1), self.part(color, 0))
@@ -100,7 +105,8 @@
     def arrived(self, step):
         for color in range(2):
             for way in range(2):
-                self.pending[(color, step, way)].wait_recv()
+                if (color, step, way) in self.pending:
+                    self.pending[(color, step, way)].wait_recv()
 
     def sent(self):
         for op in self.pending.values():
@@ -108,8 +114,8 @@
 
 
 class Reduce:
-    def __init__(self, plane, buf, base, count, lands, send, recv, chunk):
-        self.plane, self.buf, self.chunk = plane, buf, chunk
+    def __init__(self, plane, buf, base, count, lands, send, recv, chunk, direct=False):
+        self.plane, self.buf, self.chunk, self.direct = plane, buf, chunk, direct
         self.send, self.recv = send, recv
         self.half = count // 2
         self.quarter = count // 4
@@ -144,7 +150,13 @@
             ahead, behind = plane.neighbour(dim, 1), plane.neighbour(dim, -1)
             if step == 2:
                 self.fold(color)
-            if step % 2 == 0:
+            if self.direct and step >= 2:
+                if step == 2:
+                    shifts = ((3, 0, 1), (3, 1, -1), (2, 0, 2))
+                    for slot, way, shift in shifts:
+                        block = view(self.buf, dim, plane.at(dim, shift), self.rows(color))
+                        self.go(color, slot, way, block, plane.neighbour(dim, shift))
+            elif step % 2 == 0:
                 opposite = plane.at(dim, 2)
                 self.go(color, step, 0, view(self.buf, dim, opposite, self.part(color, 0)), ahead)
                 self.go(color, step, 1, view(self.buf, dim, opposite, self.part(color, 1)), behind)
@@ -172,14 +184,17 @@
         near = 1 - color
         own = plane.one(self.buf, near, plane.pos[near], self.rows(color))
         first, second = self.land(color, 3, 0), self.land(color, 3, 1)
-        return own[...].astype(jnp.float32) + first[...].astype(jnp.float32) + second[...].astype(jnp.float32)
+        value = own[...].astype(jnp.float32) + first[...].astype(jnp.float32) + second[...].astype(jnp.float32)
+        if self.direct:
+            value = value + self.land(color, 2, 0)[...].astype(jnp.float32)
+        return value
 
     def sent(self):
         for op in self.pending.values():
             op.wait_send()
 
 
-MIX_CHUNKS = 1
+MIX_CHUNKS = 3
 TOK = 192
 HALO = 32
 PAD_TOK = 256
@@ -187,12 +202,12 @@
 WIDE = SIDE * SIDE * LANES
 
 
-def land_shapes(chunks, count):
+def land_shapes(chunks, count, direct=False):
     half, quarter = count // 2, count // 4
     return [
         pltpu.VMEM((chunks, 2, 2, SIDE, quarter, LANES), jnp.bfloat16),
         pltpu.VMEM((chunks, 2, 2, SIDE, half, LANES), jnp.bfloat16),
-        pltpu.VMEM((chunks, 2, 2, quarter, LANES), jnp.bfloat16),
+        pltpu.VMEM((chunks, 2, 2, half if direct else quarter, LANES), jnp.bfloat16),
         pltpu.VMEM((chunks, 2, 2, half, LANES), jnp.bfloat16),
     ]
 
@@ -211,10 +226,11 @@
     gate_hbm,
     up_hbm,
     down_hbm,
-    chan_gain,
-    mix_gain,
-    norm_gain,
-    routes,
+    chan_hbm,
+    mix_hbm,
+    norm_hbm,
+    ids_hbm,
+    weights_hbm,
     result,
     value,
     gating,
@@ -225,6 +241,11 @@
     gate,
     up,
     down,
+    chan_gain,
+    mix_gain,
+    norm_gain,
+    ids,
+    weights,
     padded,
     halo,
     conv,
@@ -300,6 +321,11 @@
             (gate_hbm.at[0], gate),
             (up_hbm.at[0], up),
             (down_hbm.at[0], down),
+            (chan_hbm, chan_gain),
+            (mix_hbm, mix_gain),
+            (norm_hbm, norm_gain),
+            (ids_hbm, ids),
+            (weights_hbm, weights),
         )
     ):
         fetch = pltpu.make_async_copy(src, dst, fetch_sem.at[i])
@@ -307,8 +333,8 @@
         fetches.append(fetch)
 
     def mixer_table():
-        packed = routes[...]
-        turned = jnp.concatenate([packed, jnp.zeros((LANES - 8, PAD_TOK), f32)], axis=0).T
+        packed = jnp.concatenate([ids[...].astype(f32), weights[...], jnp.zeros((LANES - 8, TOK), f32)], axis=0)
+        turned = jnp.concatenate([packed, jnp.zeros((LANES, PAD_TOK - TOK), f32)], axis=1).T
         lanes_e = iota((TOK, E), 1).astype(f32)
         member = jnp.zeros((TOK, E), f32)
         weight = jnp.zeros((TOK, E), f32)
@@ -330,11 +356,11 @@
                 held[:, g * LANES : (g + 1) * LANES] = jnp.where(mine, wide, 0.0).astype(bf16)
 
     def picker_table():
-        packed = routes[...]
+        packed = ids[...].astype(f32)
         tall_e = iota((E, TOK), 0).astype(f32)
         member = jnp.zeros((E, TOK), f32)
         for k in range(TOPK):
-            member = jnp.where(packed[k : k + 1, :TOK] == tall_e, 1.0, member)
+            member = jnp.where(packed[k : k + 1, :] == tall_e, 1.0, member)
         after = (iota((TOK, TOK), 0) < iota((TOK, TOK), 1)).astype(f32).astype(bf16)
         place = jnp.dot(member.astype(bf16), after, preferred_element_type=f32)
         place = jnp.where(member > 0.0, place, -1.0)
@@ -349,7 +375,7 @@
             part = slice(b * LANES, (b + 1) * LANES)
             scaled_out[part, :] = (outw[part, :].astype(f32) * columns[:, b : b + 1]).astype(bf16)
 
-    for i in range(3):
+    for i in (0, 1, 2, 9, 10, 11, 12, 13):
         fetches[i].wait()
     unit = value[...].astype(f32) * jax.nn.sigmoid(gating[...].astype(f32))
     padded[HALO:, :] = unit.astype(bf16).astype(f32)
@@ -389,9 +415,9 @@
     spread = jnp.sum(centred * centred, axis=1, keepdims=True)
     lane = iota((TOK, LANES), 1)
     both = jnp.where(lane == 0, mean, jnp.where(lane == 1, spread, 0.0))
-    both = jnp.concatenate([both, jnp.zeros((PAD_TOK - TOK, LANES), f32)], axis=0).T[:8, :]
+    both = jnp.concatenate([both, jnp.zeros((PAD_TOK - TOK, LANES), f32)], axis=0).T[:4, :]
     gain_row = jnp.concatenate([norm_gain[...], norm_gain[...]], axis=1)
-    message[...] = jnp.where(iota((8, PAD_TOK), 0) == 2, gain_row, both)
+    message[...] = jnp.where(iota((4, PAD_TOK), 0) == 2, gain_row, both)
     me = y * SIDE + x
     for mate in mates:
         copy_to(message, stats.at[me], stat_send, stat_recv, mate).start()
@@ -424,8 +450,8 @@
             mix_part[b // SIDE, b % SIDE, :, :] = pair[:, k * LANES : (k + 1) * LANES]
     mlands = (mland0, mland1, mland2, mland3)
     count = TOK // MIX_CHUNKS
-    mreduces = [Reduce(plane, mix_part, c * count, count, mlands, mrs_send, mrs_recv, c) for c in range(MIX_CHUNKS)]
-    mgathers = [Gather(plane, mix_rows, c * count, count, mag_send, mag_recv, c) for c in range(MIX_CHUNKS)]
+    mreduces = [Reduce(plane, mix_part, c * count, count, mlands, mrs_send, mrs_recv, c, True) for c in range(MIX_CHUNKS)]
+    mgathers = [Gather(plane, mix_rows, c * count, count, mag_send, mag_recv, c, True) for c in range(MIX_CHUNKS)]
     for step in range(4):
         for c in range(MIX_CHUNKS):
             mreduces[c].issue(step)
@@ -444,18 +470,20 @@
         mgathers[c].issue(2)
     for c in range(MIX_CHUNKS):
         mgathers[c].issue(3)
+    fetches[5].wait()
     for c in range(MIX_CHUNKS):
         mgathers[c].arrived(3)
-
-    squares = jnp.zeros((TOK, LANES), f32)
-    for b in range(SIDE * SIDE):
-        block = mix_rows[b // SIDE, b % SIDE].astype(f32)
-        squares = squares + block * block
-    scale = lax.rsqrt(jnp.sum(squares, axis=1, keepdims=True) / WIDE + epsilon)
-    left = jnp.concatenate([mix_rows[b // SIDE, b % SIDE] for b in range(SIDE * SIDE)], axis=1)
-    branch = jnp.dot(left, scaled_out[...], preferred_element_type=f32) * scale
-    fetches[5].wait()
-    mid[...] = (resid[...].astype(f32) + branch).astype(bf16)
+        part = pl.ds(c * count, count)
+        squares = jnp.zeros((count, LANES), f32)
+        pieces = []
+        for b in range(SIDE * SIDE):
+            piece = mix_rows[b // SIDE, b % SIDE, part, :]
+            pieces.append(piece)
+            squares = squares + piece.astype(f32) * piece.astype(f32)
+        scale = lax.rsqrt(jnp.sum(squares, axis=1, keepdims=True) / WIDE + epsilon)
+        left = jnp.concatenate(pieces, axis=1)
+        branch = jnp.dot(left, scaled_out[...], preferred_element_type=f32) * scale
+        mid[part, :] = (resid[part, :].astype(f32) + branch).astype(bf16)
     picked = jnp.dot(picker[...], mid[...], preferred_element_type=f32).astype(bf16)
     outgoing[...] = picked.reshape(E, CAP, LANES)
 
@@ -491,7 +519,7 @@
     def compute(c):
         gathers[c].arrived(3)
         if c == 0:
-            for fetch in fetches[6:]:
+            for fetch in fetches[6:9]:
                 fetch.wait()
         step = 32
 
@@ -550,7 +578,7 @@
         finish,
     ]
     for slot in range(CHUNKS + len(stages) - 1):
-        for stage in (0, 1, 2, 3, 5, 6, 7, 8, 4):
+        for stage in range(len(stages)):
             c = slot - stage
             if 0 <= c < CHUNKS:
                 stages[stage](c)
@@ -587,8 +615,6 @@
     up_experts,
     down_experts,
 ):
-    routes = jnp.concatenate([route_ids.T.astype(jnp.float32), route_weights.T], axis=0)
-    routes = jnp.pad(routes, ((0, 0), (0, PAD_TOK - TOK)))
     vmem = pl.BlockSpec(memory_space=pltpu.VMEM)
     hbm = pl.BlockSpec(memory_space=pltpu.HBM)
     f32, bf16 = jnp.float32, jnp.bfloat16
@@ -598,19 +624,27 @@
     one = pltpu.SemaphoreType.DMA
     fed = (conv_value, conv_gate, depth_kernel, resid, point_weight, out_weight)
     experts = (gate_experts, up_experts, down_experts)
+    small = (
+        chan_gain.reshape(1, LANES),
+        mix_gain.reshape(SIDE * SIDE, LANES),
+        norm_gain.reshape(1, LANES),
+        route_ids.T,
+        route_weights.T,
+    )
     return pl.pallas_call(
         layer_kernel,
         out_shape=jax.ShapeDtypeStruct(resid.shape, bf16),
-        in_specs=[hbm] * 9 + [vmem] * 4,
+        in_specs=[hbm] * 14,
         out_specs=vmem,
         scratch_shapes=[
             *(pltpu.VMEM(a.shape, a.dtype) for a in fed),
             *(pltpu.VMEM(a.shape[1:], a.dtype) for a in experts),
+            *(pltpu.VMEM(a.shape, a.dtype) for a in small),
             pltpu.VMEM((HALO + TOK, LANES), f32),
             pltpu.VMEM((HALO, LANES), f32),
             pltpu.VMEM((TOK, LANES), f32),
-            pltpu.VMEM((8, PAD_TOK), f32),
-            pltpu.VMEM((SIDE * SIDE, 8, PAD_TOK), f32),
+            pltpu.VMEM((4, PAD_TOK), f32),
+            pltpu.VMEM((SIDE * SIDE, 4, PAD_TOK), f32),
             pltpu.VMEM((SIDE * SIDE, LANES), f32),
             pltpu.VMEM((depth, LANES), bf16),
             pltpu.VMEM((ROWS, TOK), bf16),
@@ -620,14 +654,14 @@
             pltpu.VMEM((E, CAP, LANES), bf16),
             pltpu.VMEM((SIDE, SIDE, TOK, LANES), bf16),
             pltpu.VMEM((SIDE, SIDE, TOK, LANES), bf16),
-            *land_shapes(MIX_CHUNKS, TOK // MIX_CHUNKS),
+            *land_shapes(MIX_CHUNKS, TOK // MIX_CHUNKS, True),
             pltpu.VMEM((SIDE, SIDE, ROWS, LANES), bf16),
             pltpu.VMEM((SIDE * SIDE, CROWS, LANES), bf16),
             pltpu.VMEM((SIDE, SIDE, ROWS, LANES), bf16),
             *land_shapes(CHUNKS, CROWS),
             pltpu.VMEM((ROWS, LANES), bf16),
             pltpu.VMEM((E, CAP, LANES), bf16),
-            one((9,)),
+            one((14,)),
             pltpu.SemaphoreType.REGULAR((3,)),
             one,
             one,
@@ -660,10 +694,7 @@
         gate_experts,
         up_experts,
         down_experts,
-        chan_gain.reshape(1, LANES),
-        mix_gain.reshape(SIDE * SIDE, LANES),
-        norm_gain.reshape(1, LANES),
-        routes,
+        *small,
     )
 
 

time: 134 us -> 118 us (0.88)
  Pallas kernels: 130 us -> 116 us
  local copies, waits for them, and re-layouts: 2.79 us -> 1.42 us
    pallas_call x1, Pallas kernels: 130 us -> 116 us  [shards(): pl.pallas_call(layer_kernel, out_shape=jax.ShapeDtypeStruct(resid.shape,...]
    unnamed x5 -> x1, local copies, waits for them, and re-layouts: 2.79 us -> 1.42 us
where the time goes in v4:
time: 118 us
  Pallas kernels  116 us (98%)
  local copies, waits for them, and re-layouts  1.42 us (1%)
    pallas_call x1, Pallas kernels, shards(): pl.pallas_call(layer_kernel, out_shape=jax.ShapeDtypeStruct(resid.shape,...  116 us

profile of v4, /device:TPU:1, one launch (start us, length us, event | category | flops | bytes accessed | tf_op | source)
XLA Modules:
  0.0 117.6 jit_solution(16783701606965830847)
XLA Ops:
  0.0 116.2 %layer.1 = bf16[192,128]{1,0:T(8,128)(2,1)} custom-call(bf16[192,128]{1,0:T(8,128)(2,1)} %value_hbm.1, bf16[192,128]{1,0:T(8,128)(2,1)} %gating_hbm.1, f32[31,128]{1,0:T(8,128)} %taps_hbm.1, bf16[192,128]{1,0:T(8,128)(2,1)} %resid_hbm.1, bf16[128,2048]{1,0:T(8,128)(2,1)} %point_hbm.1, bf16[2048,128]{1,0:T(8,128)(2,1)} %outw_hbm.1, ...), custom_call_target="tpu_custom_call" | custom-call | tf_op jit(solution)/shard_map/layer/pallas_call | solution.py:634
  116.2 1.4 %copy.16 = bf16[192,128]{1,0:T(8,128)(2,1)} copy(bf16[192,128]{1,0:T(8,128)(2,1)} %layer.1) | data formatting | bytes 98304

commit v5 on v4

--- a/solution.py
+++ b/solution.py
@@ -551,18 +551,19 @@
         half = CROWS // 2
         for color in range(2):
             total[pl.ds(c * CROWS + color * half, half), :] = reduces[c].total(color).astype(bf16)
-        for p in range(c * PERCHUNK, (c + 1) * PERCHUNK):
-            i, way = p // 2, p % 2
-            if i == 0 and way == 1:
-                continue
-            chip = lax.rem(z + OFFSETS[i] + CHIPS, CHIPS)
-            if i == 0:
-                target = 2 * chip + other
-                src = total.at[pl.ds(pl.multiple_of(other * CAP, CAP), CAP), :]
-            else:
-                target = 2 * chip + way
-                src = total.at[pl.ds(p * CAP, CAP), :]
-            copy_to(src, back.at[sp], back_send, back_recv, {"sp": target}).start()
+            first = c * PERCHUNK + color * PERCHUNK // 2
+            for p in range(first, first + PERCHUNK // 2):
+                i, way = p // 2, p % 2
+                if i == 0 and way == 1:
+                    continue
+                chip = lax.rem(z + OFFSETS[i] + CHIPS, CHIPS)
+                if i == 0:
+                    target = 2 * chip + other
+                    src = total.at[pl.ds(pl.multiple_of(other * CAP, CAP), CAP), :]
+                else:
+                    target = 2 * chip + way
+                    src = total.at[pl.ds(p * CAP, CAP), :]
+                copy_to(src, back.at[sp], back_send, back_recv, {"sp": target}).start()
         if c == 0:
             back[sp] = total[own_place, :]
 

time: 118 us -> 117 us (level)
  no operation moved by 1% of the time
where the time goes in v5:
time: 117 us
  Pallas kernels  116 us (99%)
  local copies, waits for them, and re-layouts  1.42 us (1%)
    pallas_call x1, Pallas kernels, shards(): pl.pallas_call(layer_kernel, out_shape=jax.ShapeDtypeStruct(resid.shape,...  116 us

profile of v5, /device:TPU:1, one launch (start us, length us, event | category | flops | bytes accessed | tf_op | source)
XLA Modules:
  0.0 117.3 jit_solution(10367464226320184577)
XLA Ops:
  0.0 115.9 %layer.1 = bf16[192,128]{1,0:T(8,128)(2,1)} custom-call(bf16[192,128]{1,0:T(8,128)(2,1)} %value_hbm.1, bf16[192,128]{1,0:T(8,128)(2,1)} %gating_hbm.1, f32[31,128]{1,0:T(8,128)} %taps_hbm.1, bf16[192,128]{1,0:T(8,128)(2,1)} %resid_hbm.1, bf16[128,2048]{1,0:T(8,128)(2,1)} %point_hbm.1, bf16[2048,128]{1,0:T(8,128)(2,1)} %outw_hbm.1, ...), custom_call_target="tpu_custom_call" | custom-call | tf_op jit(solution)/shard_map/layer/pallas_call | solution.py:635
  115.9 1.4 %copy.16 = bf16[192,128]{1,0:T(8,128)(2,1)} copy(bf16[192,128]{1,0:T(8,128)(2,1)} %layer.1) | data formatting | bytes 98304
